TPU v7x, 256 devices: a whole 4x4x8 slice. The times are simulated.
256 devices in a mesh: ep: 64 (over z, y, core), tp: 4 (over x).
Axes of the slice: x: 4, y: 4, z: 8, core: 2. Of those that a mesh axis runs over, the one named last changes fastest.
Arguments:
- queries: bfloat16 [16384, 2048], P('ep', 'tp'), may hold values from -150 to 150, as said below
- keys: bfloat16 [16384, 512], P('ep', 'tp'), may hold values from -6 to 6
- values: bfloat16 [16384, 512], P('ep', 'tp'), may hold values from -6 to 6
- cum_gates: float32 [16384, 16], P('ep', 'tp'), may hold values from -16384 to 0, as said below
- out_proj: bfloat16 [2048, 4096], P('tp'), may hold values from -0.125 to 0.125
- tokens: bfloat16 [8192, 4096], P('ep'), may hold values from -6 to 6
- norm_gain: float32 [4096], replicated, may hold values from 0.1 to 1.9
- routes: int32 [8192, 4], P('ep'), may hold values from 0 to 63, all different within a row; in each aligned block of 128 rows (0 to 127, 128 to 255, ...) at most 16 rows name the same one
- route_weights: float32 [8192, 4], P('ep'), may hold values from 0.2 to 1
- w_gate: bfloat16 [64, 4096, 1024], P('ep', None, 'tp'), may hold values from -0.09375 to 0.09375
- w_up: bfloat16 [64, 4096, 1024], P('ep', None, 'tp'), may hold values from -0.09375 to 0.09375
- w_down: bfloat16 [64, 1024, 4096], P('ep', 'tp'), may hold values from -0.1875 to 0.1875
Outputs:
- attn_mixed: bfloat16 [16384, 4096], P(('ep', 'tp'))
- moe_out: bfloat16 [8192, 4096], P('ep', 'tp')
Inputs may be any that keep to these rules, and one draw needn't show every extreme that they name: keys and queries are of order one except where the draw sets a few queries far larger. `cum_gates`: never rises along positions. `routes`: each row names 4 different experts; among the rows of one index of ep no expert is named by more than 16 rows, a bound that some block reaches in some of them.
All inputs are finite; a program needn't handle non-finite values.
Results may differ from a plain program's by a relative error of at most 0.0109.
Values may be sent and summed in bfloat16 or wider, within the bound.
A program may use at most 128 MiB of HBM per device.

v0:
```python
import math

import jax
import jax.numpy as jnp
from jax import lax
from jax.sharding import PartitionSpec as P

HD = 128


SCORE_FLOOR = -1e30


def laid_out(pieces, dim):
    pieces = jnp.moveaxis(pieces, 0, dim)
    shape = pieces.shape
    return pieces.reshape(*shape[:dim], shape[dim] * shape[dim + 1], *shape[dim + 2 :])


def copy_for_each(x, axis):
    length = lax.axis_size(axis)
    return lax.all_to_all(jnp.broadcast_to(x[None], (length, *x.shape)), axis, 0, 0, tiled=True)


def gathered_copies(x, axis, dim):
    return laid_out(copy_for_each(x, axis), dim)


def attend(queries, keys, values, cum_gates, out_proj):
    local_rows = queries.shape[0]
    groups = keys.shape[1] // HD
    group_ratio = cum_gates.shape[1] // groups
    score_scale = HD ** (-0.5)
    first_row = lax.axis_index("ep") * local_rows
    last_row = first_row + local_rows - 1
    query_four = queries.reshape(local_rows, groups, group_ratio, HD)
    query_gate = cum_gates.reshape(local_rows, groups, group_ratio)
    query_pos = first_row + jnp.arange(local_rows, dtype=jnp.int32)
    initial = (
        jnp.full((local_rows, groups, group_ratio), SCORE_FLOOR, jnp.float32),
        jnp.zeros((local_rows, groups, group_ratio), jnp.float32),
        jnp.zeros((local_rows, groups, group_ratio, HD), jnp.float32),
    )
    key_rows = lax.all_gather(keys.astype(jnp.float32), "ep", axis=0, tiled=True).astype(
        jnp.bfloat16
    )
    value_rows = lax.all_gather(values.astype(jnp.float32), "ep", axis=0, tiled=True).astype(
        jnp.bfloat16
    )
    key_gates = lax.all_gather(cum_gates, "ep", axis=0, tiled=True)
    length = key_rows.shape[0]
    block_len = math.gcd(length, 512)

    def advance(block_index, state):
        offset = block_index * block_len

        def accumulate(current):
            maxima, totals, weighted = current
            key_block = lax.dynamic_slice_in_dim(key_rows, offset, block_len, 0).reshape(
                block_len, groups, HD
            )
            value_block = lax.dynamic_slice_in_dim(value_rows, offset, block_len, 0).reshape(
                block_len, groups, HD
            )
            gate_block = lax.dynamic_slice_in_dim(key_gates, offset, block_len, 0).reshape(
                block_len, groups, group_ratio
            )
            scores = (
                jnp.einsum(
                    "qgrd,kgd->qgrk", query_four, key_block, preferred_element_type=jnp.float32
                )
                * score_scale
            )
            scores = scores + query_gate[..., None] - jnp.transpose(gate_block, (1, 2, 0))[None]
            key_pos = offset + jnp.arange(block_len, dtype=jnp.int32)
            allowed = key_pos[None, :] <= query_pos[:, None]
            scores = jnp.where(allowed[:, None, None, :], scores, SCORE_FLOOR)
            new_max = jnp.maximum(maxima, jnp.max(scores, axis=-1))
            factor = jnp.exp(maxima - new_max)
            weights = jnp.exp(scores - new_max[..., None])
            totals = factor * totals + jnp.sum(weights, axis=-1)
            weighted = factor[..., None] * weighted + jnp.einsum(
                "qgrk,kgd->qgrd",
                weights.astype(jnp.bfloat16),
                value_block,
                preferred_element_type=jnp.float32,
            )
            return (new_max, totals, weighted)

        return lax.cond(offset <= last_row, accumulate, lambda kept_state: kept_state, state)

    maxima, totals, weighted = lax.fori_loop(0, length // block_len, advance, initial)
    heads_out = (
        (weighted / totals[..., None])
        .astype(jnp.bfloat16)
        .reshape(local_rows, groups * group_ratio * HD)
    )
    return lax.psum_scatter(
        jnp.dot(heads_out, out_proj, preferred_element_type=jnp.float32).astype(jnp.bfloat16),
        "tp",
        scatter_dimension=0,
        tiled=True,
    )


def experts_part(tokens, norm_gain, routes, route_weights, w_gate, w_up, w_down):
    row_count = tokens.shape[0]
    feature_count = tokens.shape[1]
    top_count = routes.shape[1]
    experts = w_gate.shape[0] * lax.axis_size("ep")
    tp_count = lax.axis_size("tp")
    capacity = 2 * row_count * top_count // experts
    tokens_wide = tokens.astype(jnp.float32)
    normed = (
        tokens_wide
        * lax.rsqrt(jnp.mean(tokens_wide * tokens_wide, axis=-1, keepdims=True) + 1e-06)
        * norm_gain
    ).astype(jnp.bfloat16)
    flat_ids = routes.reshape(-1)
    onehot = (flat_ids[:, None] == jnp.arange(experts, dtype=jnp.int32)[None, :]).astype(jnp.int32)
    slot_rank = jnp.sum((jnp.cumsum(onehot, axis=0) - 1) * onehot, axis=1)
    slot_ids = flat_ids * capacity + slot_rank
    owner_row = jnp.arange(row_count * top_count, dtype=jnp.int32) // top_count
    slot_rows = jnp.full((experts * capacity,), -1, jnp.int32).at[slot_ids].set(owner_row)
    filled = slot_rows >= 0
    outgoing = jnp.where(
        filled[:, None], normed[jnp.maximum(slot_rows, 0)], jnp.zeros((), jnp.bfloat16)
    )
    share_size = capacity // tp_count
    blocks = outgoing.reshape(experts, capacity, feature_count)
    own_part = lax.dynamic_slice_in_dim(blocks, lax.axis_index("tp") * share_size, share_size, 1)
    partial_in = lax.all_to_all(own_part, "ep", split_axis=0, concat_axis=0, tiled=True)
    arrived = gathered_copies(partial_in, "tp", 1).reshape(-1, feature_count)
    gate_act = jnp.dot(arrived, w_gate[0], preferred_element_type=jnp.float32)
    up_act = jnp.dot(arrived, w_up[0], preferred_element_type=jnp.float32)
    latent_width = (jax.nn.silu(gate_act) * up_act).astype(jnp.bfloat16)
    partial_value = jnp.dot(latent_width, w_down[0], preferred_element_type=jnp.float32)
    results = lax.psum_scatter(
        partial_value.astype(jnp.bfloat16), "tp", scatter_dimension=1, tiled=True
    )
    returned_rows = lax.all_to_all(results, "ep", split_axis=0, concat_axis=0, tiled=True)
    picked = returned_rows[slot_ids].astype(jnp.float32).reshape(row_count, top_count, -1)
    return jnp.sum(picked * route_weights[:, :, None], axis=1).astype(jnp.bfloat16)


def per_device(
    queries,
    keys,
    values,
    cum_gates,
    out_proj,
    tokens,
    norm_gain,
    routes,
    route_weights,
    w_gate,
    w_up,
    w_down,
):
    mixed = attend(queries, keys, values, cum_gates, out_proj)
    routed = experts_part(tokens, norm_gain, routes, route_weights, w_gate, w_up, w_down)
    return (mixed, routed)


def solution(mesh):
    placed = (
        P("ep", "tp"),
        P("ep", "tp"),
        P("ep", "tp"),
        P("ep", "tp"),
        P("tp", None),
        P("ep", None),
        P(),
        P("ep", None),
        P("ep", None),
        P("ep", None, "tp"),
        P("ep", None, "tp"),
        P("ep", "tp", None),
    )
    return jax.shard_map(
        per_device,
        mesh=mesh,
        in_specs=placed,
        out_specs=(P(("ep", "tp"), None), P("ep", "tp")),
        check_vma=False,
    )
```

profile of v0, /device:TPU:224, one launch (start us, length us, event | category | flops | bytes accessed | tf_op | source)
XLA Modules:
  0.0 474.4 jit_solution(11770704548429622099)
XLA Ops:
  8.1 1.7 copy.28
  13.4 2.4 scatter_custom_fusion
  19.0 7.7 %gather_fusion = bf16[1024,4096]{1,0:T(8,128)(2,1)} fusion(bf16[128,4096]{1,0:T(8,128)(2,1)S(1)} %fusion.19, s32[1024]{0:T(1024)S(1)} %maximum_clamp_fusion), kind=kCustom, calls=%fused_computation | custom fusion | bytes 16781312 | tf_op jit(solution)/shard_map/gather | solution.py:127
  26.8 3.9 dynamic-slice_select_fusion
  30.7 64.0 %all_to_all.22 = bf16[64,4,4096]{2,1,0:T(4,128)(2,1)} all-to-all(bf16[64,4,4096]{2,1,0:T(4,128)(2,1)S(1)} %dynamic-slice_select_fusion), channel_id=1, replica_groups=mesh['ep'=64,'tp'=4] {'ep'}, dimensions={0} | all-to-all | bytes 4194304 | tf_op jit(solution)/shard_map/all_to_all | solution.py:132
  94.7 9.4 %broadcast_in_dim.69 = bf16[4,64,4,4096]{3,2,1,0:T(4,128)(2,1)} broadcast(bf16[64,4,4096]{2,1,0:T(4,128)(2,1)} %all_to_all.22), dimensions={1,2,3} | broadcast | bytes 10485760 | tf_op jit(solution)/shard_map/broadcast_in_dim | solution.py:22
  104.1 5.7 %all-to-all-start.1 = ((bf16[4,64,4,4096]{3,2,1,0:T(4,128)(2,1)}), bf16[4,64,4,4096]{3,2,1,0:T(4,128)(2,1)}, u32[]{:S(2)}, u32[]{:S(2)}) async-start(bf16[4,64,4,4096]{3,2,1,0:T(4,128)(2,1)} %broadcast_in_dim.69), calls=%async_computation.2 | async-start | bytes 16777216 | tf_op jit(solution)/shard_map/all_to_all | solution.py:22
  110.8 93.7 %all-to-all-done.1 = bf16[4,64,4,4096]{3,2,1,0:T(4,128)(2,1)} async-done(((bf16[4,64,4,4096]{3,2,1,0:T(4,128)(2,1)}), bf16[4,64,4,4096]{3,2,1,0:T(4,128)(2,1)}, u32[]{:S(2)}, u32[]{:S(2)}) %all-to-all-start.1) | async-done | bytes 8388640 | tf_op jit(solution)/shard_map/all_to_all | solution.py:22
  204.5 8.5 %copy.34 = bf16[64,4,4,4096]{3,2,1,0:T(4,128)(2,1)} copy(bf16[64,4,4,4096]{3,2,0,1:T(4,128)(2,1)} %bitcast.22) | data formatting | bytes 16777216 | tf_op jit(solution)/shard_map/transpose | solution.py:15
  212.9 12.5 %reshape_reshape.3 = bf16[1024,4096]{1,0:T(8,128)(2,1)} reshape(bf16[64,4,4,4096]{3,2,1,0:T(4,128)(2,1)} %copy.34) | data formatting | bytes 16777216 | tf_op jit(solution)/shard_map/reshape;reshape | solution.py:133
  225.5 6.5 %fusion.23 = f32[1024,256]{1,0:T(8,128)S(1)} fusion(bf16[1024,4096]{1,0:T(8,128)(2,1)} %reshape_reshape.3, bf16[1,4096,256]{2,1,0:T(8,128)(2,1)} %param.25), kind=kOutput, calls=%fused_computation.40 | convolution fusion | flops 2147483648 | bytes 11534336 | tf_op jit(solution)/shard_map/dot_general | solution.py:134
  232.4 2.4 fusion.28
  234.8 5.6 %convolution_convert_fusion = bf16[1024,4096]{1,0:T(8,128)(2,1)} fusion(bf16[1024,256]{1,0:T(8,128)(2,1)S(1)} %fusion.28, bf16[1,256,4096]{2,1,0:T(8,128)(2,1)S(1)} %copy-done), kind=kOutput, calls=%fused_computation.29 | convolution fusion | flops 2151677952 | bytes 11010048 | tf_op jit(solution)/shard_map/dot_general | solution.py:137
  241.6 43.7 %all_gather.10 = f32[16384,4]{0,1:T(4,128)S(1)} all-gather(f32[256,4]{0,1:T(4,128)S(1)} %copy-done.4), channel_id=1, replica_groups=mesh['ep'=64,'tp'=4] {'ep'}, dimensions={0}, use_global_device_ids=true | all-gather | bytes 266240 | tf_op jit(solution)/shard_map/all_gather | solution.py:50
  285.4 106.5 %while.18 = (s32[]{:T(128)}, f32[256,1,4]{0,2,1:T(4,128)S(1)}, f32[256,1,4]{0,2,1:T(4,128)S(1)}, f32[256,1,4,128]{0,3,2,1:T(8,128)S(1)}, s32[]{:T(128)}, /*index...) while((s32[]{:T(128)}, f32[256,1,4]{0,2,1:T(4,128)S(1)}, ...), condition=%wide.region_5.6_spmd.clone, body=%wide.region_0.5_spmd.clone.sunk | while | flops 273551104 | bytes 8229213 | solution.py:92
  285.4 3.6 conditional.3
  285.7 1.6 fusion.39
  289.1 3.6 conditional.3
  292.8 3.6 conditional.3
  296.4 3.6 conditional.3
  296.7 1.6 fusion.39
  300.1 3.6 conditional.3
  303.8 3.6 conditional.3
  304.0 1.6 fusion.39
  307.5 3.6 conditional.3
  307.7 1.6 fusion.39
  311.1 3.6 conditional.3
  314.8 3.6 conditional.3
  318.5 3.6 conditional.3
  318.7 1.6 fusion.39
  322.1 3.6 conditional.3
  322.3 1.6 fusion.39
  325.8 3.6 conditional.3
  329.5 3.6 conditional.3
  333.1 3.6 conditional.3
  333.3 1.6 fusion.39
  336.8 3.6 conditional.3
  337.0 1.6 fusion.39
  340.5 3.6 conditional.3
  344.1 3.6 conditional.3
  347.8 3.6 conditional.3
  348.0 1.6 fusion.39
  351.4 3.6 conditional.3
  351.7 1.6 fusion.39
  355.1 3.6 conditional.3
  358.8 3.6 conditional.3
  362.4 3.6 conditional.3
  362.6 1.6 fusion.39
  366.1 3.6 conditional.3
  366.3 1.6 fusion.39
  369.8 3.6 conditional.3
  373.4 3.6 conditional.3
  377.1 3.6 conditional.3
  377.3 1.6 fusion.39
  380.8 3.6 conditional.3
  381.0 1.6 fusion.39
  384.4 3.6 conditional.3
  388.1 3.6 conditional.3
  392.0 16.4 %all-to-all-start.2 = ((bf16[64,16,1024]{2,1,0:T(8,128)(2,1)}), bf16[64,16,1024]{2,1,0:T(8,128)(2,1)}, u32[]{:S(2)}, u32[]{:S(2)}) async-start(bf16[64,16,1024]{2,1,0:T(8,128)(2,1)} %bitcast.89), calls=%async_computation.4 | async-start | bytes 4194304 | tf_op jit(solution)/shard_map/all_to_all | solution.py:141
  408.7 4.8 %convolution_convert_fusion.1 = bf16[256,4096]{1,0:T(8,128)(2,1)} fusion(bf16[256,512]{0,1:T(8,128)(2,1)S(1)} %bitcast.90, bf16[512,4096]{1,0:T(8,128)(2,1)} %param.20), kind=kOutput, calls=%fused_computation.30 | convolution fusion | flops 1074790400 | bytes 6553600 | tf_op jit(solution)/shard_map/dot_general | solution.py:99
  414.3 42.7 %all-to-all-done.2 = bf16[64,16,1024]{2,1,0:T(8,128)(2,1)} async-done(((bf16[64,16,1024]{2,1,0:T(8,128)(2,1)}), bf16[64,16,1024]{2,1,0:T(8,128)(2,1)}, u32[]{:S(2)}, u32[]{:S(2)}) %all-to-all-start.2) | async-done | bytes 2097184 | tf_op jit(solution)/shard_map/all_to_all | solution.py:141
  457.0 4.6 gather_fusion.1
  461.6 1.7 reshape.151
  463.3 3.7 multiply_reduce_fusion
  (366 shorter events, 91.8 us)
Async XLA Ops:
  8.0 226.8 %copy-start = (bf16[1,256,4096]{2,1,0:T(8,128)(2,1)S(1)}, bf16[1,256,4096]{2,1,0:T(8,128)(2,1)}, u32[]{:S(2)}) copy-start(bf16[1,256,4096]{2,1,0:T(8,128)(2,1)} %param.27) | copy-start | bytes 6291460
  8.0 9.5 %copy-start.3 = (f32[4096]{0:T(1024)S(1)}, f32[4096]{0:T(1024)}, u32[]{:S(2)}) copy-start(f32[4096]{0:T(1024)} %param.22) | copy-start | bytes 49156
  8.0 277.3 %all-gather.5.cloned.1.call-start = ((), (), s32[]{:S(2)}) async-start(), calls=%async_computation.6 | async-start | bytes 4259840 | tf_op jit(solution)/shard_map/all_gather | solution.py:47
  104.1 100.4 %all-to-all-start.1 = ((bf16[4,64,4,4096]{3,2,1,0:T(4,128)(2,1)}), bf16[4,64,4,4096]{3,2,1,0:T(4,128)(2,1)}, u32[]{:S(2)}, u32[]{:S(2)}) async-start(bf16[4,64,4,4096]{3,2,1,0:T(4,128)(2,1)} %broadcast_in_dim.69), calls=%async_computation.2 | async-start | bytes 16777216 | tf_op jit(solution)/shard_map/all_to_all | solution.py:22
  109.8 175.6 %all-gather.3.cloned.1.call-start = ((), (), s32[]{:S(2)}) async-start(), calls=%async_computation.5 | async-start | bytes 4259840 | tf_op jit(solution)/shard_map/all_gather | solution.py:44
  110.5 281.4 %reduce-scatter.5.cloned.1.call-start = ((), (), s32[]{:S(2)}) async-start(), calls=%async_computation.8 | async-start | bytes 10485760 | tf_op jit(solution)/shard_map/reduce_scatter | solution.py:138
  225.4 6.5 %copy-start.1 = (bf16[1024,4096]{1,0:T(8,128)(2,1)S(1)}, bf16[1024,4096]{1,0:T(8,128)(2,1)}, u32[]{:S(2)}) copy-start(bf16[1024,4096]{1,0:T(8,128)(2,1)} %reshape_reshape.3) | copy-start | bytes 25165828
  225.5 7.0 %copy-start.6 = (bf16[1,4096,256]{2,1,0:T(8,128)(2,1)S(1)}, bf16[1,4096,256]{2,1,0:T(8,128)(2,1)}, u32[]{:S(2)}) copy-start(bf16[1,4096,256]{2,1,0:T(8,128)(2,1)} %param.26) | copy-start | bytes 6291460
  240.4 0.9 copy-start.2
  240.4 1.3 copy-start.4
  392.0 65.0 %all-to-all-start.2 = ((bf16[64,16,1024]{2,1,0:T(8,128)(2,1)}), bf16[64,16,1024]{2,1,0:T(8,128)(2,1)}, u32[]{:S(2)}, u32[]{:S(2)}) async-start(bf16[64,16,1024]{2,1,0:T(8,128)(2,1)} %bitcast.89), calls=%async_computation.4 | async-start | bytes 4194304 | tf_op jit(solution)/shard_map/all_to_all | solution.py:141
  408.4 58.6 %reduce-scatter.3.cloned.1.call-start = ((), (), s32[]{:S(2)}) async-start(), calls=%async_computation.7 | async-start | bytes 2621440 | tf_op jit(solution)/shard_map/reduce_scatter | solution.py:98
  413.5 0.7 copy-start.5
Sparse Core Ops, SparseCore 0:
  12.0 93.9 all-gather.4
  113.4 77.8 all-gather.2
Sparse Core Ops, SparseCore 1:
  240.5 79.7 reduce-scatter.4
  413.6 31.8 reduce-scatter.2
where the time goes:
time: 482 us; the launch traced here: 474 us
  waiting for transfers between devices  137 us (28%)
  blocking collectives  108 us (22%)
  matrix products  108 us (22%)
  local copies, waits for them, and re-layouts  53.1 us (11%)
  other arithmetic  26.5 us (5%)
  starting transfers between devices  22.6 us (5%)
  between operations  15.7 us (3%)
    all_to_all x1, waiting for transfers between devices, copy_for_each(): lax.all_to_all(jnp.broadcast_to(x[None], (length, *x.shape)), axis, 0, 0,...  93.7 us
    all_to_all x1, blocking collectives, experts_part(): lax.all_to_all(own_part, 'ep', split_axis=0, concat_axis=0, tiled=True)  64 us
    dot_general x29, matrix products, accumulate(): jnp.einsum('qgrd,kgd->qgrk', query_four, key_block, preferred_element_typ...  44.9 us
    dot_general x29, matrix products, accumulate(): jnp.einsum('qgrk,kgd->qgrd', weights.astype(jnp.bfloat16), value_block, p...  43.8 us
    all_gather x1, blocking collectives, attend(): key_gates = lax.all_gather(cum_gates, 'ep', axis=0, tiled=True)  43.7 us
    all_to_all x1, waiting for transfers between devices, experts_part(): lax.all_to_all(results, 'ep', split_axis=0, concat_axis=0, tiled=True)  42.7 us
    all_to_all x1, starting transfers between devices, experts_part(): lax.all_to_all(results, 'ep', split_axis=0, concat_axis=0, tiled=True)  16.4 us
    another operation x1, local copies, waits for them, and re-layouts, experts_part(): arrived = gathered_copies(partial_in, 'tp', 1).reshape(-1, feature_count)  12.5 us
  transfers between devices with their start and end apart: 6, of which 2 were waited for; matrix products, arithmetic and copies ran while one was open for 39% of the time, Pallas kernels for 0%

commit v1 on v0

v1 whole, which is shorter than its diff:
```python
import functools
import math

import jax
import jax.numpy as jnp
from jax import lax
from jax.experimental import pallas as pl
from jax.experimental.pallas import tpu as pltpu
from jax.sharding import PartitionSpec as P

HD = 128
CAP = 16
NYC = 8
LOG2E = math.log2(math.e)
MESH = pl.DeviceIdType.MESH
F32 = jnp.float32
BF16 = jnp.bfloat16
FLOOR = -1e30


def iota(shape, dim):
    return lax.broadcasted_iota(jnp.int32, shape, dim)


def dot(a, b):
    return jnp.dot(a, b, preferred_element_type=F32)


def experts_kernel(
    nz, nk, nx,
    tok_ref, gain_ref, routes_ref, routes_t_ref, rw_ref, wg_hbm, wu_hbm, wd_hbm,
    o_ref,
    wg, wu, wd, out, arr, part, half_in, quart_in, res, ret, c_hi, c_lo,
    w_sem, a2a_send, a2a_recv, ag_send, ag_recv, fw_send, fw_recv,
    hs_send, hs_recv, qa_send, qa_recv, qb_send, qb_recv, ret_send, ret_recv,
):
    e = lax.axis_index("ep")
    x = lax.axis_index("tp")
    n_ep = nz * nk
    z, k_own = e // nk, e % nk
    right, left, far = (x + 1) % nx, (x + nx - 1) % nx, (x + 2) % nx
    rows, width = tok_ref.shape
    quarter = width // nx
    chunk_rows = nk * CAP
    half = chunk_rows // 2

    barrier = pltpu.get_barrier_semaphore()

    @pl.loop(1, n_ep)
    def _(k):
        pl.semaphore_signal(barrier, inc=1, device_id=((e + k) % n_ep, x), device_id_type=MESH)

    for side in (left, right):
        pl.semaphore_signal(barrier, inc=1, device_id=(e, side), device_id_type=MESH)

    loads = [
        pltpu.make_async_copy(src, dst, w_sem.at[i])
        for i, (src, dst) in enumerate(((wg_hbm, wg), (wu_hbm, wu), (wd_hbm, wd)))
    ]
    for load in loads:
        load.start()

    rt = routes_t_ref[...]
    e_row = iota((n_ep, rows), 0)
    named = jnp.zeros((n_ep, rows), F32)
    for k in range(rt.shape[0]):
        named = named + (rt[k : k + 1, :] == e_row).astype(F32)
    before = (iota((rows, rows), 0) < iota((rows, rows), 1)).astype(BF16)
    named = named.astype(BF16)
    rank = dot(named, before).astype(BF16)

    tokens = tok_ref[...].astype(F32)
    inv = lax.rsqrt(jnp.mean(tokens * tokens, axis=-1, keepdims=True) + 1e-06)
    mine = pl.ds(pl.multiple_of(x * quarter, quarter), quarter)
    normed = (tok_ref[:, mine].astype(F32) * inv * gain_ref[:, mine]).astype(BF16)

    @pl.loop(0, nz)
    def _(block):
        base = block * chunk_rows
        slot = iota((chunk_rows, n_ep), 0) + base
        spread = ((slot // CAP) == iota((chunk_rows, n_ep), 1)).astype(BF16)
        hit = (dot(spread, named) > 0.5) & (
            dot(spread, rank) == ((iota((chunk_rows, rows), 0) + base) % CAP).astype(F32)
        )
        at = pl.ds(pl.multiple_of(base, chunk_rows), chunk_rows)
        out[at, :] = dot(hit.astype(BF16), normed).astype(BF16)

    pl.semaphore_wait(barrier, n_ep - 1 + 2)

    def dz_of(c):
        return jnp.where(c % 2 == 1, (c + 1) // 2, (nz - c // 2) % nz)

    def slot_rows(index):
        return pl.ds(pl.multiple_of(index * CAP, CAP), CAP)

    @pl.loop(0, nz)
    def _(c):
        dest_z = (z + dz_of(c)) % nz

        @pl.loop(jnp.where(c == 0, 1, 0), nk)
        def _(k):
            dest = dest_z * nk + (k_own + k) % nk
            pltpu.make_async_remote_copy(
                out.at[slot_rows(dest)],
                arr.at[x, c, slot_rows(k_own)],
                a2a_send.at[c],
                a2a_recv.at[c],
                device_id=(dest, x),
                device_id_type=MESH,
            ).start()

    arr[x, 0, slot_rows(k_own), :] = out[slot_rows(e), :]

    routes = routes_ref[...]
    e_col = iota((rows, n_ep), 1)
    named2 = jnp.zeros((rows, n_ep), F32)
    weight = jnp.zeros((rows, n_ep), F32)
    for k in range(routes.shape[1]):
        hit = routes[:, k : k + 1] == e_col
        named2 = named2 + hit.astype(F32)
        weight = weight + jnp.where(hit, rw_ref[:, k : k + 1], 0.0)
    named2 = named2.astype(BF16)
    earlier = (iota((rows, rows), 1) < iota((rows, rows), 0)).astype(BF16)
    rank2 = dot(earlier, named2).astype(BF16)
    w_hi = weight.astype(BF16)
    w_lo = (weight - w_hi.astype(F32)).astype(BF16)

    slot = iota((n_ep, n_ep * CAP), 1)
    spread = ((slot // CAP) == iota((n_ep, n_ep * CAP), 0)).astype(BF16)
    keep = (dot(named2, spread) > 0.5) & (
        dot(rank2, spread) == (iota((rows, n_ep * CAP), 1) % CAP).astype(F32)
    )
    c_hi[...] = jnp.where(keep, dot(w_hi, spread), 0.0).astype(BF16)
    c_lo[...] = jnp.where(keep, dot(w_lo, spread), 0.0).astype(BF16)

    def await_bytes(ref, sem):
        pltpu.make_async_copy(ref, ref, sem).wait()

    def send(src, dst, send_sem, recv_sem, to):
        pltpu.make_async_remote_copy(
            src, dst, send_sem, recv_sem, device_id=(e, to), device_id_type=MESH
        ).start()

    low, high = pl.ds(0, half), pl.ds(half, half)
    first_rows = pl.ds(0, (nk - 1) * CAP)

    @pl.loop(0, nz + 4)
    def _(step):
        @pl.when(step < nz)
        def _():
            c = step

            @pl.when(c == 0)
            def _():
                await_bytes(arr.at[x, 0, first_rows], a2a_recv.at[0])

            @pl.when(c > 0)
            def _():
                await_bytes(arr.at[x, c], a2a_recv.at[c])

            send(arr.at[x, c], arr.at[x, c], ag_send.at[0, c], ag_recv.at[0, c], right)
            send(arr.at[x, c], arr.at[x, c], ag_send.at[1, c], ag_recv.at[1, c], left)

        @pl.when((step >= 1) & (step < nz + 1))
        def _():
            c = step - 1
            await_bytes(arr.at[left, c], ag_recv.at[0, c])
            send(arr.at[left, c, low], arr.at[left, c, low], fw_send.at[0, c], fw_recv.at[0, c], right)
            await_bytes(arr.at[right, c], ag_recv.at[1, c])
            send(arr.at[right, c, high], arr.at[right, c, high], fw_send.at[1, c], fw_recv.at[1, c], left)

        @pl.when(step == 2)
        def _():
            for load in loads:
                load.wait()

        @pl.when((step >= 2) & (step < nz + 2))
        def _():
            c = step - 2
            await_bytes(arr.at[far, c, low], fw_recv.at[0, c])
            await_bytes(arr.at[far, c, high], fw_recv.at[1, c])
            gate = jnp.zeros((chunk_rows, wg.shape[1]), F32)
            up = jnp.zeros((chunk_rows, wg.shape[1]), F32)
            for q in range(nx):
                rows_q = arr[q, c]
                gate = gate + dot(rows_q, wg[q * quarter : (q + 1) * quarter, :])
                up = up + dot(rows_q, wu[q * quarter : (q + 1) * quarter, :])
            hidden = (gate * jax.nn.sigmoid(gate) * up).astype(BF16)
            for q in range(nx):
                part[q, c] = dot(hidden, wd[:, q * quarter : (q + 1) * quarter]).astype(BF16)
            send(part.at[far, c, low], half_in.at[0, c], hs_send.at[0, c], hs_recv.at[0, c], right)
            send(part.at[far, c, high], half_in.at[1, c], hs_send.at[1, c], hs_recv.at[1, c], left)
            send(part.at[right, c, high], quart_in.at[0, c, high], qa_send.at[0, c], qa_recv.at[0, c], right)
            send(part.at[left, c, low], quart_in.at[1, c, low], qa_send.at[1, c], qa_recv.at[1, c], left)

        @pl.when((step >= 3) & (step < nz + 3))
        def _():
            c = step - 3
            await_bytes(half_in.at[0, c], hs_recv.at[0, c])
            part[right, c, 0:half, :] = (
                part[right, c, 0:half, :].astype(F32) + half_in[0, c].astype(F32)
            ).astype(BF16)
            send(part.at[right, c, low], quart_in.at[0, c, low], qb_send.at[0, c], qb_recv.at[0, c], right)
            await_bytes(half_in.at[1, c], hs_recv.at[1, c])
            part[left, c, half:, :] = (
                part[left, c, half:, :].astype(F32) + half_in[1, c].astype(F32)
            ).astype(BF16)
            send(part.at[left, c, high], quart_in.at[1, c, high], qb_send.at[1, c], qb_recv.at[1, c], left)

        @pl.when(step >= 4)
        def _():
            c = step - 4
            await_bytes(quart_in.at[0, c, high], qa_recv.at[0, c])
            await_bytes(quart_in.at[1, c, low], qa_recv.at[1, c])
            await_bytes(quart_in.at[0, c, low], qb_recv.at[0, c])
            await_bytes(quart_in.at[1, c, high], qb_recv.at[1, c])
            res[c] = (
                part[x, c].astype(F32) + quart_in[0, c].astype(F32) + quart_in[1, c].astype(F32)
            ).astype(BF16)
            home_z = (z + nz - dz_of(c)) % nz

            @pl.loop(jnp.where(c == 0, 1, 0), nk)
            def _(k):
                k_home = (k_own + k) % nk
                pltpu.make_async_remote_copy(
                    res.at[c, slot_rows(k_home)],
                    ret.at[slot_rows(e)],
                    ret_send.at[c],
                    ret_recv,
                    device_id=(home_z * nk + k_home, x),
                    device_id_type=MESH,
                ).start()

    ret[slot_rows(e), :] = res[0, slot_rows(k_own), :]
    await_bytes(ret.at[pl.ds(0, (n_ep - 1) * CAP)], ret_recv)
    o_ref[...] = (dot(c_hi[...], ret[...]) + dot(c_lo[...], ret[...])).astype(BF16)

    await_bytes(res.at[0, first_rows], ret_send.at[0])
    await_bytes(arr.at[0, 0, first_rows], a2a_send.at[0])

    @pl.loop(1, nz)
    def _(c):
        await_bytes(res.at[c], ret_send.at[c])
        await_bytes(arr.at[0, c], a2a_send.at[c])

    @pl.loop(0, nz)
    def _(c):
        for side in (0, 1):
            await_bytes(arr.at[0, c], ag_send.at[side, c])
            for sem in (fw_send, hs_send, qa_send, qb_send):
                await_bytes(half_in.at[side, c], sem.at[side, c])


def experts_part(tokens, norm_gain, routes, route_weights, w_gate, w_up, w_down):
    rows, width = tokens.shape
    n_ep, nx = lax.axis_size("ep"), lax.axis_size("tp")
    nk = NYC
    nz = n_ep // nk
    quarter = width // nx
    hidden = w_gate.shape[2]
    chunk = nk * CAP
    slots = n_ep * CAP
    vmem = pl.BlockSpec(memory_space=pltpu.VMEM)
    anywhere = pl.BlockSpec(memory_space=pl.ANY)
    dma = pltpu.SemaphoreType.DMA
    pair = dma((2, nz))
    return pl.pallas_call(
        functools.partial(experts_kernel, nz, nk, nx),
        out_shape=jax.ShapeDtypeStruct((rows, quarter), BF16),
        in_specs=[vmem] * 5 + [anywhere] * 3,
        out_specs=vmem,
        scratch_shapes=[
            pltpu.VMEM((width, hidden), BF16),
            pltpu.VMEM((width, hidden), BF16),
            pltpu.VMEM((hidden, width), BF16),
            pltpu.VMEM((slots, quarter), BF16),
            pltpu.VMEM((nx, nz, chunk, quarter), BF16),
            pltpu.VMEM((nx, nz, chunk, quarter), BF16),
            pltpu.VMEM((2, nz, chunk // 2, quarter), BF16),
            pltpu.VMEM((2, nz, chunk, quarter), BF16),
            pltpu.VMEM((nz, chunk, quarter), BF16),
            pltpu.VMEM((slots, quarter), BF16),
            pltpu.VMEM((rows, slots), BF16),
            pltpu.VMEM((rows, slots), BF16),
            dma((3,)),
            dma((nz,)),
            dma((nz,)),
            pair, pair, pair, pair, pair, pair, pair, pair, pair, pair,
            dma((nz,)),
            dma,
        ],
        compiler_params=pltpu.CompilerParams(
            collective_id=0, has_side_effects=True, vmem_limit_bytes=58 * 2**20
        ),
        cost_estimate=pl.CostEstimate(
            flops=100 * 10**9, bytes_accessed=10 * 2**20, transcendentals=0
        ),
    )(
        tokens,
        norm_gain[None],
        routes,
        routes.T,
        route_weights,
        w_gate[0],
        w_up[0],
        w_down[0],
    )


def flash_kernel(q_ref, kvg_ref, own_ref, o_ref, m_ref, l_ref, acc_ref):
    e = lax.axis_index("ep")
    rows = q_ref.shape[0]
    heads = q_ref.shape[1] // HD
    m_ref[...] = jnp.full_like(m_ref, FLOOR)
    l_ref[...] = jnp.zeros_like(l_ref)
    acc_ref[...] = jnp.zeros_like(acc_ref)
    halves = rows // 128
    ratio = HD ** (-0.5) * LOG2E
    base = own_ref[...][:, 0:1] * 1.0

    def visit(j, masked):
        key = kvg_ref[pl.ds(2 * j, 2), 0:rows, :].reshape(2 * rows, HD)
        value = kvg_ref[pl.ds(2 * j, 2), rows : 2 * rows, :].reshape(2 * rows, HD)
        pieces = kvg_ref[pl.ds(2 * j, 2), 2 * rows :, :].astype(F32)
        n = heads * halves
        gates = pieces[:, 0:n] + pieces[:, n : 2 * n] + pieces[:, 2 * n : 3 * n]
        if masked:
            pos = j * 2 * rows + iota((rows, 2 * rows), 1)
            own_pos = e * rows + iota((rows, 2 * rows), 0)
            allowed = pos <= own_pos
        for h in range(heads):
            line = jnp.concatenate(
                [gates[b, h * halves + i : h * halves + i + 1, :] for b in range(2) for i in range(halves)],
                axis=1,
            )
            line = (line - base[h * halves : h * halves + 1, :]) * LOG2E
            s = lax.dot_general(
                q_ref[:, h * HD : (h + 1) * HD], key, (((1,), (1,)), ((), ())), preferred_element_type=F32
            )
            t = s * ratio - line
            if masked:
                t = jnp.where(allowed, t, FLOOR)
            old = m_ref[h]
            new = jnp.maximum(old, jnp.max(t, axis=1, keepdims=True))
            alpha = jnp.exp2(old - new)
            w = jnp.exp2(t - new)
            l_ref[h] = alpha * l_ref[h] + jnp.sum(w, axis=1, keepdims=True)
            acc_ref[h] = alpha * acc_ref[h] + dot(w.astype(BF16), value)
            m_ref[h] = new

    @pl.loop(0, e // 2)
    def _(j):
        visit(j, False)

    visit(e // 2, True)
    for h in range(heads):
        o_ref[:, h * HD : (h + 1) * HD] = (acc_ref[h] / l_ref[h]).astype(BF16)


def attend(queries, keys, values, cum_gates, out_proj, experts):
    rows = queries.shape[0]
    heads = cum_gates.shape[1]
    lines = cum_gates.T.reshape(heads * rows // 128, 128)
    hi = lax.reduce_precision(lines, 8, 7)
    mid = lax.reduce_precision(lines - hi, 8, 7)
    lo = lines - hi - mid
    pieces = jnp.concatenate([hi, mid, lo], axis=0).astype(BF16)
    packed = jnp.concatenate([keys, values, pieces], axis=0)
    gathered = lax.all_gather(packed, "ep", axis=0, tiled=False)
    gathered, routed = lax.optimization_barrier((gathered, experts))
    vmem = pl.BlockSpec(memory_space=pltpu.VMEM)
    heads_out = pl.pallas_call(
        flash_kernel,
        out_shape=jax.ShapeDtypeStruct(queries.shape, BF16),
        in_specs=[vmem] * 3,
        out_specs=vmem,
        scratch_shapes=[
            pltpu.VMEM((heads, rows, 1), F32),
            pltpu.VMEM((heads, rows, 1), F32),
            pltpu.VMEM((heads, rows, HD), F32),
        ],
        compiler_params=pltpu.CompilerParams(vmem_limit_bytes=40 * 2**20),
        cost_estimate=pl.CostEstimate(
            flops=20 * 10**9, bytes_accessed=10 * 2**20, transcendentals=16 * 2**20
        ),
    )(queries, gathered, lines)
    mixed = lax.psum_scatter(
        jnp.dot(heads_out, out_proj, preferred_element_type=F32).astype(BF16),
        "tp",
        scatter_dimension=0,
        tiled=True,
    )
    return (mixed, routed)


def per_device(
    queries, keys, values, cum_gates, out_proj,
    tokens, norm_gain, routes, route_weights, w_gate, w_up, w_down,
):
    routed = experts_part(tokens, norm_gain, routes, route_weights, w_gate, w_up, w_down)
    return attend(queries, keys, values, cum_gates, out_proj, routed)


def solution(mesh):
    placed = (
        P("ep", "tp"), P("ep", "tp"), P("ep", "tp"), P("ep", "tp"), P("tp", None),
        P("ep", None), P(), P("ep", None), P("ep", None),
        P("ep", None, "tp"), P("ep", None, "tp"), P("ep", "tp", None),
    )
    return jax.shard_map(
        per_device,
        mesh=mesh,
        in_specs=placed,
        out_specs=(P(("ep", "tp"), None), P("ep", "tp")),
        check_vma=False,
    )
```

time: 482 us -> 302 us (0.63)
  Pallas kernels: 0 us -> 236 us
  blocking collectives: 108 us -> 0 us
  matrix products: 108 us -> 2.61 us
  waiting for transfers between devices: 137 us -> 35.3 us
  local copies, waits for them, and re-layouts: 53.1 us -> 10.1 us
  other arithmetic: 26.5 us -> 0.04 us
  starting transfers between devices: 22.6 us -> 0.08 us
    pallas_call x0 -> x2, Pallas kernels: none -> 236 us  [the longest x1 183 us: experts_part(): pl.pallas_call(functools.partial(experts_kernel, nz, nk, nx), out_shape=j...]
    all_to_all x2 -> x0, waiting for transfers between devices: 136 us -> none  [the longest x1 93.7 us: copy_for_each(): lax.all_to_all(jnp.broadcast_to(x[None], (length, *x.shape)), axis, 0, 0,...]
    dot_general x62 -> x1, matrix products: 108 us -> 2.61 us  [attend(): jnp.dot(heads_out, out_proj, preferred_element_type=F32).astype(BF16)]
    all_to_all x1 -> x0, blocking collectives: 64 us -> none  [experts_part(): lax.all_to_all(own_part, 'ep', split_axis=0, concat_axis=0, tiled=True)]
    all_gather x1 -> x0, blocking collectives: 43.7 us -> none  [attend(): key_gates = lax.all_gather(cum_gates, 'ep', axis=0, tiled=True)]
    reduce_scatter x2 -> x1, waiting for transfers between devices: 0.03 us -> 35.2 us  [attend(): lax.psum_scatter(jnp.dot(heads_out, out_proj, preferred_element_type=F32)...]
    all_to_all x2 -> x0, starting transfers between devices: 22.1 us -> none  [the longest x1 16.4 us: experts_part(): lax.all_to_all(results, 'ep', split_axis=0, concat_axis=0, tiled=True)]
    reduce_sum x32 -> x0, other arithmetic: 13.9 us -> none  [the longest x29 8.61 us: accumulate(): totals = factor * totals + jnp.sum(weights, axis=-1)]
  transfers between devices with their start and end apart: 6 -> 2, of which waited for: 2 -> 1; matrix products, arithmetic and copies ran while one was open for 39% -> 1% of each run, Pallas kernels for 0% -> 62%
where the time goes in v1:
time: 302 us; the launch traced here: 298 us
  Pallas kernels  236 us (78%)
  waiting for transfers between devices  35.3 us (12%)
  between operations  14.1 us (5%)
  local copies, waits for them, and re-layouts  10.1 us (3%)
    pallas_call x1, Pallas kernels, experts_part(): pl.pallas_call(functools.partial(experts_kernel, nz, nk, nx), out_shape=j...  183 us
    pallas_call x1, Pallas kernels, attend(): pl.pallas_call(flash_kernel, out_shape=jax.ShapeDtypeStruct(queries.shape...  52.3 us
    reduce_scatter x1, waiting for transfers between devices, attend(): lax.psum_scatter(jnp.dot(heads_out, out_proj, preferred_element_type=F32)...  35.2 us
    unnamed x15, local copies, waits for them, and re-layouts  9.39 us
  transfers between devices with their start and end apart: 2, of which 1 were waited for; matrix products, arithmetic and copies ran while one was open for 1% of the time, Pallas kernels for 62%

profile of v1, /device:TPU:224, one launch (start us, length us, event | category | flops | bytes accessed | tf_op | source)
XLA Modules:
  0.0 298.0 jit_solution(17084633181203129333)
XLA Ops:
  7.2 0.0 all-gather.3.cloned.1.call-start
  7.2 0.7 reshape.7.own_ref
  7.9 0.8 constant_dynamic-update-slice_fusion.4
  8.7 0.9 constant_dynamic-update-slice_fusion.3
  9.6 0.0 copy-start.2
  9.7 0.6 copy-done.2
  10.3 0.0 all-gather.3.cloned.1.call-update
  10.3 0.0 reduce-scatter.2.cloned.1.call-start
  10.4 1.4 copy.15.rw_ref
  11.8 1.4 copy.14.routes_ref
  13.2 0.0 copy-start.1
  13.2 183.5 %shard_map.131 = bf16[128,1024]{1,0:T(8,128)(2,1)} custom-call(bf16[128,4096]{1,0:T(8,128)(2,1)} %tok_ref.1, f32[1,4096]{1,0:T(1,128)} %bitcast.15, s32[128,4]{1,0:T(8,128)} %copy.14.routes_ref, s32[4,128]{1,0:T(4,128)} %bitcast.11, f32[128,4]{1,0:T(8,128)} %copy.15.rw_ref, bf16[4096,256]{1,0:T(8,128)(2,1)} %bitcast.12, bf16[4096,256]{1,0:T(8,128)(2,1)} %bitcast.13, ...), custom_call_target="tpu_custom_call" | custom-call | flops 99999997952 | bytes 10485760 | tf_op jit(solution)/shard_map/pallas_call | solution.py:267
  196.7 0.0 all-gather.3.cloned.1.call-done
  196.7 0.0 copy-done.1
  196.7 0.0 copy-start
  196.7 3.5 %copy-done = bf16[34304,128]{1,0:T(8,128)(2,1)S(1)} copy-done((bf16[34304,128]{1,0:T(8,128)(2,1)S(1)}, bf16[34304,128]{1,0:T(8,128)(2,1)}, u32[]{:S(2)}) %copy-start) | copy-done | bytes 8781848
  200.2 0.0 copy-start.4
  200.2 52.3 %shard_map.132 = bf16[256,512]{1,0:T(8,128)(2,1)S(1)} custom-call(bf16[256,512]{1,0:T(8,128)(2,1)S(1)} %copy-done.1, bf16[64,536,128]{2,1,0:T(8,128)(2,1)S(1)} %bitcast.9, f32[8,128]{1,0:T(8,128)S(1)} %reshape.7.own_ref), custom_call_target="tpu_custom_call" | custom-call | flops 20000000000 | bytes 10485760 | tf_op jit(solution)/shard_map/pallas_call | solution.py:372
  252.5 0.0 copy-done.4
  252.5 0.0 copy-start.3
  252.6 2.6 convolution_convert_fusion
  255.2 0.0 reduce-scatter.2.cloned.1.call-update
  255.2 35.2 %reduce-scatter.2.cloned.1.call-done = bf16[64,4096]{1,0:T(8,128)(2,1)} async-done(((bf16[256,4096]{1,0:T(8,128)(2,1)}), bf16[64,4096]{1,0:T(8,128)(2,1)}) %reduce-scatter.2.cloned.1.call-update) | async-done | bytes 524304 | tf_op jit(solution)/shard_map/reduce_scatter | solution.py:387
  290.4 0.0 copy-done.3
  290.4 0.7 copy.21
  (3 shorter events, 0.0 us)
Async XLA Ops:
  7.2 189.5 %all-gather.3.cloned.1.call-start = ((), (), s32[]{:S(2)}) async-start(), calls=%async_computation.2 | async-start | bytes 8919040 | tf_op jit(solution)/shard_map/all_gather | solution.py:369
  9.6 0.7 copy-start.2
  10.3 280.1 %reduce-scatter.2.cloned.1.call-start = ((), (), s32[]{:S(2)}) async-start(), calls=%async_computation.1 | async-start | bytes 2621440 | tf_op jit(solution)/shard_map/reduce_scatter | solution.py:387
  13.2 183.5 %copy-start.1 = (bf16[256,512]{1,0:T(8,128)(2,1)S(1)}, bf16[256,512]{1,0:T(8,128)(2,1)}, u32[]{:S(2)}) copy-start(bf16[256,512]{1,0:T(8,128)(2,1)} %q_ref.1) | copy-start | bytes 786436
  196.7 3.5 %copy-start = (bf16[34304,128]{1,0:T(8,128)(2,1)S(1)}, bf16[34304,128]{1,0:T(8,128)(2,1)}, u32[]{:S(2)}) copy-start(bf16[34304,128]{1,0:T(8,128)(2,1)} %all-gather.3.cloned.1.call-done) | copy-start | bytes 26345476
  200.2 52.3 %copy-start.4 = (bf16[512,4096]{1,0:T(8,128)(2,1)S(1)}, bf16[512,4096]{1,0:T(8,128)(2,1)}, u32[]{:S(2)}) copy-start(bf16[512,4096]{1,0:T(8,128)(2,1)} %param.16) | copy-start | bytes 12582916
  252.5 37.9 %copy-start.3 = (bf16[128,1024]{1,0:T(8,128)(2,1)S(1)}, bf16[128,1024]{1,0:T(8,128)(2,1)}, u32[]{:S(2)}) copy-start(bf16[128,1024]{1,0:T(8,128)(2,1)} %shard_map.131) | copy-start | bytes 786436
Sparse Core Ops, SparseCore 0:
  11.3 88.9 all-gather.2
  255.3 35.0 reduce-scatter.1

commit v2 on v1

v2 whole, which is shorter than its diff:
```python
import functools
import math

import jax
import jax.numpy as jnp
from jax import lax
from jax.experimental import pallas as pl
from jax.experimental.pallas import tpu as pltpu
from jax.sharding import PartitionSpec as P

HD = 128
CAP = 16
NYC = 8
LOG2E = math.log2(math.e)
MESH = pl.DeviceIdType.MESH
F32 = jnp.float32
BF16 = jnp.bfloat16
FLOOR = -1e30
AHEAD = 4


def iota(shape, dim):
    return lax.broadcasted_iota(jnp.int32, shape, dim)


def dot(a, b):
    return jnp.dot(a, b, preferred_element_type=F32)


def step_kernel(
    nz, nk, nx,
    tok_ref, gain_ref, routes_ref, routes_t_ref, rw_ref, q_ref, lines_ref,
    wg_hbm, wu_hbm, wd_hbm, wo_hbm, key_hbm, value_hbm,
    mixed_ref, o_ref,
    wg, wu, wd, wo, out, arr, part, half_in, quart_in, ret, c_hi, c_lo,
    kv, m_ref, l_ref, acc_ref, heads_ref,
    w_sem, a2a_send, a2a_recv, ag_send, ag_recv, fw_send, fw_recv,
    hs_send, hs_recv, qa_send, qa_recv, qb_send, qb_recv, ret_send, ret_recv,
    kz_send, kz_recv, ky_send, ky_recv, kf_send, kf_recv, ks_send, ks_recv,
):
    e = lax.axis_index("ep")
    x = lax.axis_index("tp")
    n_ep = nz * nk
    ny = nk // 2
    z, k_own = e // nk, e % nk
    y, core = k_own // 2, k_own % 2
    right, left, far = (x + 1) % nx, (x + nx - 1) % nx, (x + 2) % nx
    rows, width = tok_ref.shape
    quarter = width // nx
    chunk_rows = nk * CAP
    half = chunk_rows // 2
    q_rows = q_ref.shape[0]
    heads = q_ref.shape[1] // HD
    block_rows = kv.shape[2]

    barrier = pltpu.get_barrier_semaphore()

    @pl.loop(1, n_ep)
    def _(k):
        pl.semaphore_signal(barrier, inc=1, device_id=((e + k) % n_ep, x), device_id_type=MESH)

    for side in (left, right):
        pl.semaphore_signal(barrier, inc=1, device_id=(e, side), device_id_type=MESH)

    own_kv = [
        pltpu.make_async_copy(key_hbm, kv.at[z, k_own, pl.ds(0, q_rows)], w_sem.at[4]),
        pltpu.make_async_copy(value_hbm, kv.at[z, k_own, pl.ds(q_rows, q_rows)], w_sem.at[5]),
    ]
    loads = [
        pltpu.make_async_copy(src, dst, w_sem.at[i])
        for i, (src, dst) in enumerate(((wg_hbm, wg), (wu_hbm, wu), (wd_hbm, wd), (wo_hbm, wo)))
    ]
    for load in own_kv + loads:
        load.start()

    lines = lines_ref[...]
    g_hi = lines.astype(BF16)
    rest = lines - g_hi.astype(F32)
    g_mid = rest.astype(BF16)
    g_lo = (rest - g_mid.astype(F32)).astype(BF16)
    n_lines = lines.shape[0]
    kv[z, k_own, 2 * q_rows :, :] = jnp.concatenate(
        [g_hi.astype(F32), g_mid.astype(F32), g_lo.astype(F32), jnp.zeros_like(lines)], axis=0
    ).astype(BF16)

    rt = routes_t_ref[...]
    e_row = iota((n_ep, rows), 0)
    named = jnp.zeros((n_ep, rows), F32)
    for k in range(rt.shape[0]):
        named = named + (rt[k : k + 1, :] == e_row).astype(F32)
    before = (iota((rows, rows), 0) < iota((rows, rows), 1)).astype(BF16)
    named = named.astype(BF16)
    rank = dot(named, before).astype(BF16)

    tokens = tok_ref[...].astype(F32)
    inv = lax.rsqrt(jnp.mean(tokens * tokens, axis=-1, keepdims=True) + 1e-06)
    mine = pl.ds(pl.multiple_of(x * quarter, quarter), quarter)
    normed = (tok_ref[:, mine].astype(F32) * inv * gain_ref[:, mine]).astype(BF16)

    @pl.loop(0, nz)
    def _(block):
        base = block * chunk_rows
        slot = iota((chunk_rows, n_ep), 0) + base
        spread = ((slot // CAP) == iota((chunk_rows, n_ep), 1)).astype(BF16)
        hit = (dot(spread, named) > 0.5) & (
            dot(spread, rank) == ((iota((chunk_rows, rows), 0) + base) % CAP).astype(F32)
        )
        at = pl.ds(pl.multiple_of(base, chunk_rows), chunk_rows)
        out[at, :] = dot(hit.astype(BF16), normed).astype(BF16)

    for load in own_kv:
        load.wait()
    pl.semaphore_wait(barrier, n_ep - 1 + 2)

    def dz_of(c):
        return jnp.where(c % 2 == 1, (c + 1) // 2, (nz - c // 2) % nz)

    def slot_rows(index):
        return pl.ds(pl.multiple_of(index * CAP, CAP), CAP)

    def await_bytes(ref, sem):
        pltpu.make_async_copy(ref, ref, sem).wait()

    def send(src, dst, send_sem, recv_sem, to):
        pltpu.make_async_remote_copy(
            src, dst, send_sem, recv_sem, device_id=(e, to), device_id_type=MESH
        ).start()

    def send_block(ref, send_sem, recv_sem, to):
        pltpu.make_async_remote_copy(
            ref, ref, send_sem, recv_sem, device_id=(to, x), device_id_type=MESH
        ).start()

    def dispatch(c):
        dest_z = (z + dz_of(c)) % nz

        @pl.loop(jnp.where(c == 0, 1, 0), nk)
        def _(k):
            dest = dest_z * nk + (k_own + k) % nk
            pltpu.make_async_remote_copy(
                out.at[slot_rows(dest)],
                arr.at[x, c, slot_rows(k_own)],
                a2a_send.at[c],
                a2a_recv.at[c],
                device_id=(dest, x),
                device_id_type=MESH,
            ).start()

    ahead = min(AHEAD, nz)

    @pl.loop(0, ahead)
    def _(c):
        dispatch(c)

    arr[x, 0, slot_rows(k_own), :] = out[slot_rows(e), :]

    routes = routes_ref[...]
    e_col = iota((rows, n_ep), 1)
    named2 = jnp.zeros((rows, n_ep), F32)
    weight = jnp.zeros((rows, n_ep), F32)
    for k in range(routes.shape[1]):
        hit = routes[:, k : k + 1] == e_col
        named2 = named2 + hit.astype(F32)
        weight = weight + jnp.where(hit, rw_ref[:, k : k + 1], 0.0)
    named2 = named2.astype(BF16)
    earlier = (iota((rows, rows), 1) < iota((rows, rows), 0)).astype(BF16)
    rank2 = dot(earlier, named2).astype(BF16)
    w_hi = weight.astype(BF16)
    w_lo = (weight - w_hi.astype(F32)).astype(BF16)

    slot = iota((n_ep, n_ep * CAP), 1)
    spread = ((slot // CAP) == iota((n_ep, n_ep * CAP), 0)).astype(BF16)
    keep = (dot(named2, spread) > 0.5) & (
        dot(rank2, spread) == (iota((rows, n_ep * CAP), 1) % CAP).astype(F32)
    )
    c_hi[...] = jnp.where(keep, dot(w_hi, spread), 0.0).astype(BF16)
    c_lo[...] = jnp.where(keep, dot(w_lo, spread), 0.0).astype(BF16)

    m_ref[...] = jnp.full_like(m_ref, FLOOR)
    l_ref[...] = jnp.zeros_like(l_ref)
    acc_ref[...] = jnp.zeros_like(acc_ref)
    halves = q_rows // 128
    ratio = HD ** (-0.5) * LOG2E

    def visit(zs, p, masked):
        both = pl.ds(2 * p, 2)
        key = kv[zs, both, 0:q_rows, :].reshape(2 * q_rows, HD)
        value = kv[zs, both, q_rows : 2 * q_rows, :].reshape(2 * q_rows, HD)
        terms = kv[zs, both, 2 * q_rows :, :].astype(F32)
        n = n_lines
        gates = terms[:, 0:n] + terms[:, n : 2 * n] + terms[:, 2 * n : 3 * n]
        if masked:
            pos = p * 2 * q_rows + iota((q_rows, 2 * q_rows), 1)
            own_pos = k_own * q_rows + iota((q_rows, 2 * q_rows), 0)
            allowed = pos <= own_pos
        for h in range(heads):
            line = jnp.concatenate(
                [gates[b, h * halves + i : h * halves + i + 1, :] for b in range(2) for i in range(halves)],
                axis=1,
            )
            line = (line - lines_ref[h * halves : h * halves + 1, 0:1]) * LOG2E
            s = lax.dot_general(
                q_ref[:, h * HD : (h + 1) * HD], key, (((1,), (1,)), ((), ())), preferred_element_type=F32
            )
            t = s * ratio - line
            if masked:
                t = jnp.where(allowed, t, FLOOR)
            old = m_ref[h]
            new = jnp.maximum(old, jnp.max(t, axis=1, keepdims=True))
            alpha = jnp.exp2(old - new)
            w = jnp.exp2(t - new)
            l_ref[h] = alpha * l_ref[h] + jnp.sum(w, axis=1, keepdims=True)
            acc_ref[h] = alpha * acc_ref[h] + dot(w.astype(BF16), value)
            m_ref[h] = new

    low, high = pl.ds(0, half), pl.ds(half, half)
    first_rows = pl.ds(0, (nk - 1) * CAP)
    b_low, b_high = pl.ds(0, block_rows // 2), pl.ds(block_rows // 2, block_rows // 2)
    y_up, y_down, y_far = (y + 1) % ny, (y + ny - 1) % ny, (y + 2) % ny
    plane = z * nk
    up_dev, down_dev = plane + y_up * 2 + core, plane + y_down * 2 + core
    sibling = plane + y * 2 + (1 - core)

    def scatter_sends(c):
        send(part.at[far, c, low], half_in.at[0, c], hs_send.at[0, c], hs_recv.at[0, c], right)
        send(part.at[far, c, high], half_in.at[1, c], hs_send.at[1, c], hs_recv.at[1, c], left)
        send(part.at[right, c, high], quart_in.at[0, c, high], qa_send.at[0, c], qa_recv.at[0, c], right)
        send(part.at[left, c, low], quart_in.at[1, c, low], qa_send.at[1, c], qa_recv.at[1, c], left)

    @pl.loop(0, nz + 6)
    def _(step):
        @pl.when(step + ahead < nz)
        def _():
            dispatch(step + ahead)

        @pl.when(step < nz)
        def _():
            c = step

            @pl.when(c == 0)
            def _():
                await_bytes(arr.at[x, 0, first_rows], a2a_recv.at[0])

            @pl.when(c > 0)
            def _():
                await_bytes(arr.at[x, c], a2a_recv.at[c])

            send(arr.at[x, c], arr.at[x, c], ag_send.at[0, c], ag_recv.at[0, c], right)
            send(arr.at[x, c], arr.at[x, c], ag_send.at[1, c], ag_recv.at[1, c], left)

        @pl.when((step < nz) & (step <= z))
        def _():
            d = step
            block = kv.at[z - d, k_own]

            @pl.when(d > 0)
            def _():
                await_bytes(block, kz_recv.at[d])

            @pl.when(z + 1 < nz)
            def _():
                send_block(block, kz_send.at[d], kz_recv.at[d + 1], e + nk)

            send_block(block, ky_send.at[0, d], ky_recv.at[0, d], up_dev)
            send_block(block, ky_send.at[1, d], ky_recv.at[1, d], down_dev)
            send_block(block, ks_send.at[0, d], ks_recv.at[0, d], sibling)

        @pl.when((step >= 1) & (step < nz + 1))
        def _():
            c = step - 1
            await_bytes(arr.at[left, c], ag_recv.at[0, c])
            send(arr.at[left, c, low], arr.at[left, c, low], fw_send.at[0, c], fw_recv.at[0, c], right)
            await_bytes(arr.at[right, c], ag_recv.at[1, c])
            send(arr.at[right, c, high], arr.at[right, c, high], fw_send.at[1, c], fw_recv.at[1, c], left)

        @pl.when((step >= 1) & (step < nz + 1) & (step - 1 <= z))
        def _():
            d = step - 1
            zs = z - d
            below = kv.at[zs, y_down * 2 + core]
            await_bytes(below, ky_recv.at[0, d])
            part_low = kv.at[zs, y_down * 2 + core, b_low]
            send_block(part_low, kf_send.at[0, d], kf_recv.at[0, d], up_dev)
            send_block(below, ks_send.at[1, d], ks_recv.at[1, d], sibling)
            above = kv.at[zs, y_up * 2 + core]
            await_bytes(above, ky_recv.at[1, d])
            part_high = kv.at[zs, y_up * 2 + core, b_high]
            send_block(part_high, kf_send.at[1, d], kf_recv.at[1, d], down_dev)
            send_block(above, ks_send.at[2, d], ks_recv.at[2, d], sibling)

        @pl.when(step == 2)
        def _():
            for load in loads[:3]:
                load.wait()

        @pl.when((step >= 2) & (step < nz + 2))
        def _():
            c = step - 2
            await_bytes(arr.at[far, c, low], fw_recv.at[0, c])
            await_bytes(arr.at[far, c, high], fw_recv.at[1, c])
            gate = jnp.zeros((chunk_rows, wg.shape[1]), F32)
            up = jnp.zeros((chunk_rows, wg.shape[1]), F32)
            for q in range(nx):
                rows_q = arr[q, c]
                gate = gate + dot(rows_q, wg[q * quarter : (q + 1) * quarter, :])
                up = up + dot(rows_q, wu[q * quarter : (q + 1) * quarter, :])
            hidden = (gate * jax.nn.sigmoid(gate) * up).astype(BF16)
            for q in range(nx):
                part[q, c] = dot(hidden, wd[:, q * quarter : (q + 1) * quarter]).astype(BF16)
            scatter_sends(c)

        @pl.when((step >= 3) & (step < nz + 5))
        def _():
            c = step - 3
            await_bytes(half_in.at[0, c], hs_recv.at[0, c])
            part[right, c, 0:half, :] = (
                part[right, c, 0:half, :].astype(F32) + half_in[0, c].astype(F32)
            ).astype(BF16)
            send(part.at[right, c, low], quart_in.at[0, c, low], qb_send.at[0, c], qb_recv.at[0, c], right)
            await_bytes(half_in.at[1, c], hs_recv.at[1, c])
            part[left, c, half:, :] = (
                part[left, c, half:, :].astype(F32) + half_in[1, c].astype(F32)
            ).astype(BF16)
            send(part.at[left, c, high], quart_in.at[1, c, high], qb_send.at[1, c], qb_recv.at[1, c], left)

        @pl.when(step >= 4)
        def _():
            c = step - 4
            await_bytes(quart_in.at[0, c, high], qa_recv.at[0, c])
            await_bytes(quart_in.at[1, c, low], qa_recv.at[1, c])
            await_bytes(quart_in.at[0, c, low], qb_recv.at[0, c])
            await_bytes(quart_in.at[1, c, high], qb_recv.at[1, c])
            part[x, c] = (
                part[x, c].astype(F32) + quart_in[0, c].astype(F32) + quart_in[1, c].astype(F32)
            ).astype(BF16)

            @pl.when(c < nz)
            def _():
                home_z = (z + nz - dz_of(c)) % nz

                @pl.loop(jnp.where(c == 0, 1, 0), nk)
                def _(k):
                    k_home = (k_own + k) % nk
                    pltpu.make_async_remote_copy(
                        part.at[x, c, slot_rows(k_home)],
                        ret.at[slot_rows(e)],
                        ret_send.at[c],
                        ret_recv,
                        device_id=(home_z * nk + k_home, x),
                        device_id_type=MESH,
                    ).start()

        @pl.when((step >= 2) & (step < nz + 2) & (step - 2 <= z))
        def _():
            d = step - 2
            zs = z - d
            opposite = y_far * 2 + core
            await_bytes(kv.at[zs, opposite, b_low], kf_recv.at[0, d])
            await_bytes(kv.at[zs, opposite, b_high], kf_recv.at[1, d])
            send_block(kv.at[zs, opposite], ks_send.at[3, d], ks_recv.at[3, d], sibling)

        @pl.when((step >= 3) & (step < nz + 3) & (step - 3 <= z))
        def _():
            d = step - 3
            zs = z - d
            for i, line_y in enumerate((y, y_down, y_up, y_far)):
                await_bytes(kv.at[zs, line_y * 2 + 1 - core], ks_recv.at[i, d])

            @pl.loop(0, jnp.where(d == 0, k_own // 2, nk // 2))
            def _(p):
                visit(zs, p, False)

            @pl.when(d == 0)
            def _():
                visit(zs, k_own // 2, True)

        @pl.when(step == nz + 2)
        def _():
            loads[3].wait()
            for h in range(heads):
                heads_ref[:, h * HD : (h + 1) * HD] = (acc_ref[h] / l_ref[h]).astype(BF16)
            for n in range(nx):
                mixed = dot(heads_ref[...], wo[:, n * quarter : (n + 1) * quarter]).astype(BF16)
                for q in range(nx):
                    part[q, nz + n // 2, n % 2 * half : n % 2 * half + half, :] = mixed[
                        q * half : (q + 1) * half, :
                    ]
            scatter_sends(nz)
            scatter_sends(nz + 1)

    for n in range(nx):
        mixed_ref[:, n * quarter : (n + 1) * quarter] = part[
            x, nz + n // 2, n % 2 * half : n % 2 * half + half, :
        ]

    ret[slot_rows(e), :] = part[x, 0, slot_rows(k_own), :]
    await_bytes(ret.at[pl.ds(0, (n_ep - 1) * CAP)], ret_recv)
    o_ref[...] = (dot(c_hi[...], ret[...]) + dot(c_lo[...], ret[...])).astype(BF16)

    await_bytes(part.at[x, 0, first_rows], ret_send.at[0])
    await_bytes(arr.at[0, 0, first_rows], a2a_send.at[0])

    @pl.loop(1, nz)
    def _(c):
        await_bytes(part.at[x, c], ret_send.at[c])
        await_bytes(arr.at[0, c], a2a_send.at[c])

    @pl.loop(0, nz)
    def _(c):
        for side in (0, 1):
            await_bytes(arr.at[0, c], ag_send.at[side, c])
            await_bytes(half_in.at[side, c], fw_send.at[side, c])

        @pl.when(c <= z)
        def _():
            block = kv.at[0, 0]

            @pl.when(z + 1 < nz)
            def _():
                await_bytes(block, kz_send.at[c])

            for side in (0, 1):
                await_bytes(block, ky_send.at[side, c])
                await_bytes(kv.at[0, 0, b_low], kf_send.at[side, c])
            for i in range(4):
                await_bytes(block, ks_send.at[i, c])

    @pl.loop(0, nz + 2)
    def _(c):
        for side in (0, 1):
            for sem in (hs_send, qa_send, qb_send):
                await_bytes(half_in.at[side, c], sem.at[side, c])


def per_device(
    queries, keys, values, cum_gates, out_proj,
    tokens, norm_gain, routes, route_weights, w_gate, w_up, w_down,
):
    rows, width = tokens.shape
    q_rows = queries.shape[0]
    heads = cum_gates.shape[1]
    n_ep, nx = lax.axis_size("ep"), lax.axis_size("tp")
    nk = NYC
    nz = n_ep // nk
    quarter = width // nx
    hidden = w_gate.shape[2]
    chunk = nk * CAP
    slots = n_ep * CAP
    lines = cum_gates.T.reshape(heads * q_rows // 128, 128)
    block_rows = 2 * q_rows + 4 * lines.shape[0]
    vmem = pl.BlockSpec(memory_space=pltpu.VMEM)
    anywhere = pl.BlockSpec(memory_space=pl.ANY)
    dma = pltpu.SemaphoreType.DMA
    pair = dma((2, nz))
    more = dma((2, nz + 2))
    line = dma((nz + 1,))
    return pl.pallas_call(
        functools.partial(step_kernel, nz, nk, nx),
        out_shape=(
            jax.ShapeDtypeStruct((q_rows // nx, width), BF16),
            jax.ShapeDtypeStruct((rows, quarter), BF16),
        ),
        in_specs=[vmem] * 7 + [anywhere] * 6,
        out_specs=(vmem, vmem),
        scratch_shapes=[
            pltpu.VMEM((width, hidden), BF16),
            pltpu.VMEM((width, hidden), BF16),
            pltpu.VMEM((hidden, width), BF16),
            pltpu.VMEM(out_proj.shape, BF16),
            pltpu.VMEM((slots, quarter), BF16),
            pltpu.VMEM((nx, nz, chunk, quarter), BF16),
            pltpu.VMEM((nx, nz + 2, chunk, quarter), BF16),
            pltpu.VMEM((2, nz + 2, chunk // 2, quarter), BF16),
            pltpu.VMEM((2, nz + 2, chunk, quarter), BF16),
            pltpu.VMEM((slots, quarter), BF16),
            pltpu.VMEM((rows, slots), BF16),
            pltpu.VMEM((rows, slots), BF16),
            pltpu.VMEM((nz, nk, block_rows, HD), BF16),
            pltpu.VMEM((heads, q_rows, 1), F32),
            pltpu.VMEM((heads, q_rows, 1), F32),
            pltpu.VMEM((heads, q_rows, HD), F32),
            pltpu.VMEM((q_rows, heads * HD), BF16),
            dma((6,)),
            dma((nz,)), dma((nz,)),
            pair, pair, pair, pair,
            more, more, more, more, more, more,
            dma((nz,)),
            dma,
            line, line, pair, pair, pair, pair, dma((4, nz)), dma((4, nz)),
        ],
        compiler_params=pltpu.CompilerParams(
            collective_id=0, has_side_effects=True, vmem_limit_bytes=67043328
        ),
        cost_estimate=pl.CostEstimate(
            flops=100 * 10**9, bytes_accessed=10 * 2**20, transcendentals=0
        ),
    )(
        tokens, norm_gain[None], routes, routes.T, route_weights, queries, lines,
        w_gate[0], w_up[0], w_down[0], out_proj, keys, values,
    )


def solution(mesh):
    placed = (
        P("ep", "tp"), P("ep", "tp"), P("ep", "tp"), P("ep", "tp"), P("tp", None),
        P("ep", None), P(), P("ep", None), P("ep", None),
        P("ep", None, "tp"), P("ep", None, "tp"), P("ep", "tp", None),
    )
    return jax.shard_map(
        per_device,
        mesh=mesh,
        in_specs=placed,
        out_specs=(P(("ep", "tp"), None), P("ep", "tp")),
        check_vma=False,
    )
```

time: 302 us -> 221 us (0.73)
  the two profiles are of different devices: /device:TPU:224 before, /device:TPU:1 now
where the time goes in v2:
time: 221 us; the launch traced here: 220 us
  Pallas kernels  212 us (96%)
  local copies, waits for them, and re-layouts  7.65 us (3%)
    pallas_call x1, Pallas kernels, per_device(): pl.pallas_call(functools.partial(step_kernel, nz, nk, nx), out_shape=(jax...  212 us
    unnamed x4, local copies, waits for them, and re-layouts  6.37 us

profile of v2, /device:TPU:1, one launch (start us, length us, event | category | flops | bytes accessed | tf_op | source)
XLA Modules:
  0.0 220.3 jit_solution(18356935800401602907)
XLA Ops:
  0.6 1.3 reshape.7.lines_ref
  1.9 1.4 copy.15.rw_ref
  3.3 1.4 copy.14.routes_ref
  4.7 212.0 %shard_map.131 = (bf16[64,4096]{1,0:T(8,128)(2,1)}, bf16[128,1024]{1,0:T(8,128)(2,1)}) custom-call(bf16[128,4096]{1,0:T(8,128)(2,1)} %tok_ref.1, f32[1,4096]{1,0:T(1,128)} %bitcast.11, s32[128,4]{1,0:T(8,128)} %copy.14.routes_ref, s32[4,128]{1,0:T(4,128)} %bitcast.7, f32[128,4]{1,0:T(8,128)} %copy.15.rw_ref, bf16[256,512]{1,0:T(8,128)(2,1)} %q_ref.1, ...), custom_call_target="tpu_custom_call" | custom-call | flops 99999997952 | bytes 10485760 | tf_op jit(solution)/shard_map/pallas_call | solution.py:457
  216.8 1.9 copy.18
  218.6 1.7 copy.19

commit v3 on v2

--- a/solution.py
+++ b/solution.py
@@ -16,7 +16,7 @@
 F32 = jnp.float32
 BF16 = jnp.bfloat16
 FLOOR = -1e30
-AHEAD = 4
+AHEAD = 2
 
 
 def iota(shape, dim):
@@ -229,64 +229,46 @@
 
     @pl.loop(0, nz + 6)
     def _(step):
-        @pl.when(step + ahead < nz)
-        def _():
-            dispatch(step + ahead)
-
-        @pl.when(step < nz)
-        def _():
-            c = step
-
-            @pl.when(c == 0)
-            def _():
-                await_bytes(arr.at[x, 0, first_rows], a2a_recv.at[0])
-
-            @pl.when(c > 0)
-            def _():
-                await_bytes(arr.at[x, c], a2a_recv.at[c])
-
-            send(arr.at[x, c], arr.at[x, c], ag_send.at[0, c], ag_recv.at[0, c], right)
-            send(arr.at[x, c], arr.at[x, c], ag_send.at[1, c], ag_recv.at[1, c], left)
-
-        @pl.when((step < nz) & (step <= z))
-        def _():
-            d = step
-            block = kv.at[z - d, k_own]
-
-            @pl.when(d > 0)
-            def _():
-                await_bytes(block, kz_recv.at[d])
-
-            @pl.when(z + 1 < nz)
-            def _():
-                send_block(block, kz_send.at[d], kz_recv.at[d + 1], e + nk)
-
-            send_block(block, ky_send.at[0, d], ky_recv.at[0, d], up_dev)
-            send_block(block, ky_send.at[1, d], ky_recv.at[1, d], down_dev)
-            send_block(block, ks_send.at[0, d], ks_recv.at[0, d], sibling)
-
-        @pl.when((step >= 1) & (step < nz + 1))
-        def _():
-            c = step - 1
-            await_bytes(arr.at[left, c], ag_recv.at[0, c])
-            send(arr.at[left, c, low], arr.at[left, c, low], fw_send.at[0, c], fw_recv.at[0, c], right)
-            await_bytes(arr.at[right, c], ag_recv.at[1, c])
-            send(arr.at[right, c, high], arr.at[right, c, high], fw_send.at[1, c], fw_recv.at[1, c], left)
-
-        @pl.when((step >= 1) & (step < nz + 1) & (step - 1 <= z))
-        def _():
-            d = step - 1
-            zs = z - d
-            below = kv.at[zs, y_down * 2 + core]
-            await_bytes(below, ky_recv.at[0, d])
-            part_low = kv.at[zs, y_down * 2 + core, b_low]
-            send_block(part_low, kf_send.at[0, d], kf_recv.at[0, d], up_dev)
-            send_block(below, ks_send.at[1, d], ks_recv.at[1, d], sibling)
-            above = kv.at[zs, y_up * 2 + core]
-            await_bytes(above, ky_recv.at[1, d])
-            part_high = kv.at[zs, y_up * 2 + core, b_high]
-            send_block(part_high, kf_send.at[1, d], kf_recv.at[1, d], down_dev)
-            send_block(above, ks_send.at[2, d], ks_recv.at[2, d], sibling)
+        @pl.when((step >= 3) & (step < nz + 5))
+        def _():
+            c = step - 3
+            await_bytes(half_in.at[0, c], hs_recv.at[0, c])
+            part[right, c, 0:half, :] = (
+                part[right, c, 0:half, :].astype(F32) + half_in[0, c].astype(F32)
+            ).astype(BF16)
+            send(part.at[right, c, low], quart_in.at[0, c, low], qb_send.at[0, c], qb_recv.at[0, c], right)
+            await_bytes(half_in.at[1, c], hs_recv.at[1, c])
+            part[left, c, half:, :] = (
+                part[left, c, half:, :].astype(F32) + half_in[1, c].astype(F32)
+            ).astype(BF16)
+            send(part.at[left, c, high], quart_in.at[1, c, high], qb_send.at[1, c], qb_recv.at[1, c], left)
+
+        @pl.when(step >= 4)
+        def _():
+            c = step - 4
+            await_bytes(quart_in.at[0, c, high], qa_recv.at[0, c])
+            await_bytes(quart_in.at[1, c, low], qa_recv.at[1, c])
+            await_bytes(quart_in.at[0, c, low], qb_recv.at[0, c])
+            await_bytes(quart_in.at[1, c, high], qb_recv.at[1, c])
+            part[x, c] = (
+                part[x, c].astype(F32) + quart_in[0, c].astype(F32) + quart_in[1, c].astype(F32)
+            ).astype(BF16)
+
+            @pl.when(c < nz)
+            def _():
+                home_z = (z + nz - dz_of(c)) % nz
+
+                @pl.loop(jnp.where(c == 0, 1, 0), nk)
+                def _(k):
+                    k_home = (k_own + k) % nk
+                    pltpu.make_async_remote_copy(
+                        part.at[x, c, slot_rows(k_home)],
+                        ret.at[slot_rows(e)],
+                        ret_send.at[c],
+                        ret_recv,
+                        device_id=(home_z * nk + k_home, x),
+                        device_id_type=MESH,
+                    ).start()
 
         @pl.when(step == 2)
         def _():
@@ -309,46 +291,43 @@
                 part[q, c] = dot(hidden, wd[:, q * quarter : (q + 1) * quarter]).astype(BF16)
             scatter_sends(c)
 
-        @pl.when((step >= 3) & (step < nz + 5))
-        def _():
-            c = step - 3
-            await_bytes(half_in.at[0, c], hs_recv.at[0, c])
-            part[right, c, 0:half, :] = (
-                part[right, c, 0:half, :].astype(F32) + half_in[0, c].astype(F32)
-            ).astype(BF16)
-            send(part.at[right, c, low], quart_in.at[0, c, low], qb_send.at[0, c], qb_recv.at[0, c], right)
-            await_bytes(half_in.at[1, c], hs_recv.at[1, c])
-            part[left, c, half:, :] = (
-                part[left, c, half:, :].astype(F32) + half_in[1, c].astype(F32)
-            ).astype(BF16)
-            send(part.at[left, c, high], quart_in.at[1, c, high], qb_send.at[1, c], qb_recv.at[1, c], left)
-
-        @pl.when(step >= 4)
-        def _():
-            c = step - 4
-            await_bytes(quart_in.at[0, c, high], qa_recv.at[0, c])
-            await_bytes(quart_in.at[1, c, low], qa_recv.at[1, c])
-            await_bytes(quart_in.at[0, c, low], qb_recv.at[0, c])
-            await_bytes(quart_in.at[1, c, high], qb_recv.at[1, c])
-            part[x, c] = (
-                part[x, c].astype(F32) + quart_in[0, c].astype(F32) + quart_in[1, c].astype(F32)
-            ).astype(BF16)
-
-            @pl.when(c < nz)
-            def _():
-                home_z = (z + nz - dz_of(c)) % nz
-
-                @pl.loop(jnp.where(c == 0, 1, 0), nk)
-                def _(k):
-                    k_home = (k_own + k) % nk
-                    pltpu.make_async_remote_copy(
-                        part.at[x, c, slot_rows(k_home)],
-                        ret.at[slot_rows(e)],
-                        ret_send.at[c],
-                        ret_recv,
-                        device_id=(home_z * nk + k_home, x),
-                        device_id_type=MESH,
-                    ).start()
+        @pl.when((step >= 1) & (step < nz + 1))
+        def _():
+            c = step - 1
+            await_bytes(arr.at[left, c], ag_recv.at[0, c])
+            send(arr.at[left, c, low], arr.at[left, c, low], fw_send.at[0, c], fw_recv.at[0, c], right)
+            await_bytes(arr.at[right, c], ag_recv.at[1, c])
+            send(arr.at[right, c, high], arr.at[right, c, high], fw_send.at[1, c], fw_recv.at[1, c], left)
+
+        @pl.when(step < nz)
+        def _():
+            c = step
+
+            @pl.when(c == 0)
+            def _():
+                await_bytes(arr.at[x, 0, first_rows], a2a_recv.at[0])
+
+            @pl.when(c > 0)
+            def _():
+                await_bytes(arr.at[x, c], a2a_recv.at[c])
+
+            send(arr.at[x, c], arr.at[x, c], ag_send.at[0, c], ag_recv.at[0, c], right)
+            send(arr.at[x, c], arr.at[x, c], ag_send.at[1, c], ag_recv.at[1, c], left)
+
+        @pl.when((step >= 3) & (step < nz + 3) & (step - 3 <= z))
+        def _():
+            d = step - 3
+            zs = z - d
+            for i, line_y in enumerate((y, y_down, y_up, y_far)):
+                await_bytes(kv.at[zs, line_y * 2 + 1 - core], ks_recv.at[i, d])
+
+            @pl.loop(0, jnp.where(d == 0, k_own // 2, nk // 2))
+            def _(p):
+                visit(zs, p, False)
+
+            @pl.when(d == 0)
+            def _():
+                visit(zs, k_own // 2, True)
 
         @pl.when((step >= 2) & (step < nz + 2) & (step - 2 <= z))
         def _():
@@ -359,20 +338,41 @@
             await_bytes(kv.at[zs, opposite, b_high], kf_recv.at[1, d])
             send_block(kv.at[zs, opposite], ks_send.at[3, d], ks_recv.at[3, d], sibling)
 
-        @pl.when((step >= 3) & (step < nz + 3) & (step - 3 <= z))
-        def _():
-            d = step - 3
+        @pl.when((step >= 1) & (step < nz + 1) & (step - 1 <= z))
+        def _():
+            d = step - 1
             zs = z - d
-            for i, line_y in enumerate((y, y_down, y_up, y_far)):
-                await_bytes(kv.at[zs, line_y * 2 + 1 - core], ks_recv.at[i, d])
-
-            @pl.loop(0, jnp.where(d == 0, k_own // 2, nk // 2))
-            def _(p):
-                visit(zs, p, False)
-
-            @pl.when(d == 0)
-            def _():
-                visit(zs, k_own // 2, True)
+            below = kv.at[zs, y_down * 2 + core]
+            await_bytes(below, ky_recv.at[0, d])
+            part_low = kv.at[zs, y_down * 2 + core, b_low]
+            send_block(part_low, kf_send.at[0, d], kf_recv.at[0, d], up_dev)
+            send_block(below, ks_send.at[1, d], ks_recv.at[1, d], sibling)
+            above = kv.at[zs, y_up * 2 + core]
+            await_bytes(above, ky_recv.at[1, d])
+            part_high = kv.at[zs, y_up * 2 + core, b_high]
+            send_block(part_high, kf_send.at[1, d], kf_recv.at[1, d], down_dev)
+            send_block(above, ks_send.at[2, d], ks_recv.at[2, d], sibling)
+
+        @pl.when((step < nz) & (step <= z))
+        def _():
+            d = step
+            block = kv.at[z - d, k_own]
+
+            @pl.when(d > 0)
+            def _():
+                await_bytes(block, kz_recv.at[d])
+
+            @pl.when(z + 1 < nz)
+            def _():
+                send_block(block, kz_send.at[d], kz_recv.at[d + 1], e + nk)
+
+            send_block(block, ky_send.at[0, d], ky_recv.at[0, d], up_dev)
+            send_block(block, ky_send.at[1, d], ky_recv.at[1, d], down_dev)
+            send_block(block, ks_send.at[0, d], ks_recv.at[0, d], sibling)
+
+        @pl.when(step + ahead < nz)
+        def _():
+            dispatch(step + ahead)
 
         @pl.when(step == nz + 2)
         def _():

time: 221 us -> 199 us (0.900)
  the two profiles are of different devices: /device:TPU:1 before, /device:TPU:224 now
where the time goes in v3:
time: 199 us; the launch traced here: 196 us
  Pallas kernels  188 us (94%)
  local copies, waits for them, and re-layouts  7.65 us (4%)
    pallas_call x1, Pallas kernels, per_device(): pl.pallas_call(functools.partial(step_kernel, nz, nk, nx), out_shape=(jax...  188 us
    unnamed x4, local copies, waits for them, and re-layouts  6.37 us

profile of v3, /device:TPU:224, one launch (start us, length us, event | category | flops | bytes accessed | tf_op | source)
XLA Modules:
  0.0 196.2 jit_solution(2082976418600255743)
XLA Ops:
  0.6 1.3 reshape.7.lines_ref
  1.9 1.4 copy.15.rw_ref
  3.3 1.4 copy.14.routes_ref
  4.7 187.9 %shard_map.131 = (bf16[64,4096]{1,0:T(8,128)(2,1)}, bf16[128,1024]{1,0:T(8,128)(2,1)}) custom-call(bf16[128,4096]{1,0:T(8,128)(2,1)} %tok_ref.1, f32[1,4096]{1,0:T(1,128)} %bitcast.11, s32[128,4]{1,0:T(8,128)} %copy.14.routes_ref, s32[4,128]{1,0:T(4,128)} %bitcast.7, f32[128,4]{1,0:T(8,128)} %copy.15.rw_ref, bf16[256,512]{1,0:T(8,128)(2,1)} %q_ref.1, ...), custom_call_target="tpu_custom_call" | custom-call | flops 99999997952 | bytes 10485760 | tf_op jit(solution)/shard_map/pallas_call | solution.py:457
  192.6 1.9 copy.18
  194.5 1.7 copy.19

commit v4 on v3

v4 whole, which is shorter than its diff:
```python
import functools
import math

import jax
import jax.numpy as jnp
from jax import lax
from jax.experimental import pallas as pl
from jax.experimental.pallas import tpu as pltpu
from jax.sharding import PartitionSpec as P

HD = 128
CAP = 16
NYC = 8
LOG2E = math.log2(math.e)
MESH = pl.DeviceIdType.MESH
F32 = jnp.float32
BF16 = jnp.bfloat16
FLOOR = -1e30
AHEAD = 2


def iota(shape, dim):
    return lax.broadcasted_iota(jnp.int32, shape, dim)


def dot(a, b):
    return jnp.dot(a, b, preferred_element_type=F32)


def step_kernel(
    nz, nk, nx,
    tok_ref, gain_ref, routes_ref, rw_ref, q_ref, gates_ref,
    wg_hbm, wu_hbm, wd_hbm, wo_hbm, key_hbm, value_hbm,
    mixed_ref, o_ref,
    wg, wu, wd, wo, out, arr, part, half_in, quart_in, ret, c_hi, c_lo,
    kv, m_ref, l_ref, acc_ref, heads_ref, norm_ref, wide,
    w_sem, a2a_send, a2a_recv, ag_send, ag_recv, fw_send, fw_recv,
    hs_send, hs_recv, qa_send, qa_recv, qb_send, qb_recv, ret_send, ret_recv,
    kz_send, kz_recv, ky_send, ky_recv, kf_send, kf_recv, ks_send, ks_recv,
):
    e = lax.axis_index("ep")
    x = lax.axis_index("tp")
    n_ep = nz * nk
    ny = nk // 2
    z, k_own = e // nk, e % nk
    y, core = k_own // 2, k_own % 2
    right, left, far = (x + 1) % nx, (x + nx - 1) % nx, (x + 2) % nx
    rows, width = tok_ref.shape
    quarter = width // nx
    chunk_rows = nk * CAP
    half = chunk_rows // 2
    q_rows = q_ref.shape[0]
    heads = q_ref.shape[1] // HD
    block_rows = kv.shape[2]

    barrier = pltpu.get_barrier_semaphore()

    @pl.loop(1, n_ep)
    def _(k):
        pl.semaphore_signal(barrier, inc=1, device_id=((e + k) % n_ep, x), device_id_type=MESH)

    for side in (left, right):
        pl.semaphore_signal(barrier, inc=1, device_id=(e, side), device_id_type=MESH)

    own_kv = [
        pltpu.make_async_copy(key_hbm, kv.at[z, k_own, pl.ds(0, q_rows)], w_sem.at[4]),
        pltpu.make_async_copy(value_hbm, kv.at[z, k_own, pl.ds(q_rows, q_rows)], w_sem.at[5]),
    ]
    loads = [
        pltpu.make_async_copy(src, dst, w_sem.at[i])
        for i, (src, dst) in enumerate(((wg_hbm, wg), (wu_hbm, wu), (wd_hbm, wd), (wo_hbm, wo)))
    ]
    for load in own_kv + loads:
        load.start()

    lines = jnp.concatenate(
        [
            gates_ref[h : h + 1, i * 128 : (i + 1) * 128]
            for h in range(heads)
            for i in range(q_rows // 128)
        ],
        axis=0,
    )
    g_hi = lines.astype(BF16)
    rest = lines - g_hi.astype(F32)
    g_mid = rest.astype(BF16)
    g_lo = (rest - g_mid.astype(F32)).astype(BF16)
    n_lines = lines.shape[0]
    kv[z, k_own, 2 * q_rows :, :] = jnp.concatenate(
        [g_hi.astype(F32), g_mid.astype(F32), g_lo.astype(F32), jnp.zeros_like(lines)], axis=0
    ).astype(BF16)

    routes = routes_ref[...]
    e_row = iota((n_ep, rows), 0)
    named = jnp.zeros((n_ep, rows), F32)
    weight = jnp.zeros((n_ep, rows), F32)
    for k in range(routes.shape[0]):
        hit = routes[k : k + 1, :] == e_row
        named = named + hit.astype(F32)
        weight = weight + jnp.where(hit, rw_ref[k : k + 1, :], 0.0)
    before = (iota((rows, rows), 0) < iota((rows, rows), 1)).astype(BF16)
    named = named.astype(BF16)
    rank = dot(named, before).astype(BF16)

    tokens = tok_ref[...].astype(F32)
    inv = lax.rsqrt(jnp.mean(tokens * tokens, axis=-1, keepdims=True) + 1e-06)
    norm_ref[...] = (tokens * inv * gain_ref[...]).astype(BF16)
    normed = norm_ref[:, pl.ds(pl.multiple_of(x * quarter, quarter), quarter)]

    def picks(base):
        slot = iota((chunk_rows, n_ep), 0) + base
        spread = ((slot // CAP) == iota((chunk_rows, n_ep), 1)).astype(BF16)
        hit = (dot(spread, named) > 0.5) & (
            dot(spread, rank) == ((iota((chunk_rows, rows), 0) + base) % CAP).astype(F32)
        )
        return hit.astype(BF16)

    order = [0, nz // 2]
    for near in range(1, (nz + 1) // 2):
        order[-1:-1] = [near, nz - near]
    if nz > 4:
        order[4], order[-1] = order[-1], order[4]

    def dz_of(c):
        return sum(jnp.where(c == i, dz, 0) for i, dz in enumerate(order))

    def prepare(c):
        base = (z + dz_of(c)) % nz * chunk_rows
        at = pl.ds(pl.multiple_of(base, chunk_rows), chunk_rows)
        out[at, :] = dot(picks(base), normed).astype(BF16)

    prepare(1)

    for load in own_kv:
        load.wait()
    pl.semaphore_wait(barrier, n_ep - 1 + 2)

    def slot_rows(index):
        return pl.ds(pl.multiple_of(index * CAP, CAP), CAP)

    def await_bytes(ref, sem):
        pltpu.make_async_copy(ref, ref, sem).wait()

    def send(src, dst, send_sem, recv_sem, to):
        pltpu.make_async_remote_copy(
            src, dst, send_sem, recv_sem, device_id=(e, to), device_id_type=MESH
        ).start()

    def send_block(ref, send_sem, recv_sem, to):
        pltpu.make_async_remote_copy(
            ref, ref, send_sem, recv_sem, device_id=(to, x), device_id_type=MESH
        ).start()

    def dispatch(c):
        dest_z = (z + dz_of(c)) % nz

        @pl.loop(0, nk)
        def _(k):
            dest = dest_z * nk + (k_own + k) % nk
            pltpu.make_async_remote_copy(
                out.at[slot_rows(dest)],
                arr.at[x, c, slot_rows(k_own)],
                a2a_send.at[c],
                a2a_recv.at[c],
                device_id=(dest, x),
                device_id_type=MESH,
            ).start()

    b_low, b_high = pl.ds(0, block_rows // 2), pl.ds(block_rows // 2, block_rows // 2)
    y_up, y_down, y_far = (y + 1) % ny, (y + ny - 1) % ny, (y + 2) % ny
    plane = z * nk
    up_dev, down_dev = plane + y_up * 2 + core, plane + y_down * 2 + core
    sibling = plane + y * 2 + (1 - core)

    def spread_column(d):
        block = kv.at[z - d, k_own]

        @pl.when(z + 1 < nz)
        def _():
            send_block(block, kz_send.at[d], kz_recv.at[d + 1], e + nk)

        send_block(block, ky_send.at[0, d], ky_recv.at[0, d], up_dev)
        send_block(block, ky_send.at[1, d], ky_recv.at[1, d], down_dev)
        send_block(block, ks_send.at[0, d], ks_recv.at[0, d], sibling)

    dispatch(1)
    spread_column(0)

    @pl.loop(2, min(AHEAD, nz - 1) + 1)
    def _(c):
        prepare(c)
        dispatch(c)

    near = picks(z * chunk_rows)
    for q in range(nx):
        wide[q] = dot(near, norm_ref[:, q * quarter : (q + 1) * quarter]).astype(BF16)

    def dispatch_near(q):
        @pl.loop(1, nk)
        def _(k):
            k_dest = (k_own + k) % nk
            pltpu.make_async_remote_copy(
                wide.at[q, slot_rows(k_dest)],
                arr.at[q, 0, slot_rows(k_own)],
                a2a_send.at[0],
                a2a_recv.at[0],
                device_id=(plane + k_dest, x),
                device_id_type=MESH,
            ).start()

    arr[:, 0, slot_rows(k_own), :] = wide[:, slot_rows(k_own), :]

    same = (iota((rows, rows), 0) == iota((rows, rows), 1)).astype(BF16)

    def turned(a):
        return lax.dot_general(
            same, a, (((1,), (1,)), ((), ())), preferred_element_type=F32
        ).astype(BF16)

    w_hi = weight.astype(BF16)
    w_lo = (weight - w_hi.astype(F32)).astype(BF16)
    slot = iota((n_ep, n_ep * CAP), 1)
    spread = ((slot // CAP) == iota((n_ep, n_ep * CAP), 0)).astype(BF16)
    keep = (dot(turned(named), spread) > 0.5) & (
        dot(turned(rank), spread) == (iota((rows, n_ep * CAP), 1) % CAP).astype(F32)
    )
    c_hi[...] = jnp.where(keep, dot(turned(w_hi), spread), 0.0).astype(BF16)
    c_lo[...] = jnp.where(keep, dot(turned(w_lo), spread), 0.0).astype(BF16)

    m_ref[...] = jnp.full_like(m_ref, FLOOR)
    l_ref[...] = jnp.zeros_like(l_ref)
    acc_ref[...] = jnp.zeros_like(acc_ref)
    halves = q_rows // 128
    ratio = HD ** (-0.5) * LOG2E

    def visit(zs, p, masked):
        both = pl.ds(2 * p, 2)
        key = kv[zs, both, 0:q_rows, :].reshape(2 * q_rows, HD)
        value = kv[zs, both, q_rows : 2 * q_rows, :].reshape(2 * q_rows, HD)
        terms = kv[zs, both, 2 * q_rows :, :].astype(F32)
        n = n_lines
        gates = terms[:, 0:n] + terms[:, n : 2 * n] + terms[:, 2 * n : 3 * n]
        if masked:
            pos = p * 2 * q_rows + iota((q_rows, 2 * q_rows), 1)
            own_pos = k_own * q_rows + iota((q_rows, 2 * q_rows), 0)
            allowed = pos <= own_pos
        for h in range(heads):
            line = jnp.concatenate(
                [gates[b, h * halves + i : h * halves + i + 1, :] for b in range(2) for i in range(halves)],
                axis=1,
            )
            line = (line - gates_ref[h : h + 1, 0:1]) * LOG2E
            s = lax.dot_general(
                q_ref[:, h * HD : (h + 1) * HD], key, (((1,), (1,)), ((), ())), preferred_element_type=F32
            )
            t = s * ratio - line
            if masked:
                t = jnp.where(allowed, t, FLOOR)
            old = m_ref[h]
            new = jnp.maximum(old, jnp.max(t, axis=1, keepdims=True))
            alpha = jnp.exp2(old - new)
            w = jnp.exp2(t - new)
            l_ref[h] = alpha * l_ref[h] + jnp.sum(w, axis=1, keepdims=True)
            acc_ref[h] = alpha * acc_ref[h] + dot(w.astype(BF16), value)
            m_ref[h] = new

    low, high = pl.ds(0, half), pl.ds(half, half)
    first_rows = pl.ds(0, (nk - 1) * CAP)
    def half_sends(c):
        send(part.at[far, c, low], half_in.at[0, c], hs_send.at[0, c], hs_recv.at[0, c], right)
        send(part.at[far, c, high], half_in.at[1, c], hs_send.at[1, c], hs_recv.at[1, c], left)

    def quarter_sends(c):
        send(part.at[right, c, high], quart_in.at[0, c, high], qa_send.at[0, c], qa_recv.at[0, c], right)
        send(part.at[left, c, low], quart_in.at[1, c, low], qa_send.at[1, c], qa_recv.at[1, c], left)

    def pass_sums(c):
        await_bytes(half_in.at[0, c], hs_recv.at[0, c])
        part[right, c, 0:half, :] = (
            part[right, c, 0:half, :].astype(F32) + half_in[0, c].astype(F32)
        ).astype(BF16)
        send(part.at[right, c, low], quart_in.at[0, c, low], qb_send.at[0, c], qb_recv.at[0, c], right)
        await_bytes(half_in.at[1, c], hs_recv.at[1, c])
        part[left, c, half:, :] = (
            part[left, c, half:, :].astype(F32) + half_in[1, c].astype(F32)
        ).astype(BF16)
        send(part.at[left, c, high], quart_in.at[1, c, high], qb_send.at[1, c], qb_recv.at[1, c], left)

    def finish(c):
        await_bytes(quart_in.at[0, c, high], qa_recv.at[0, c])
        await_bytes(quart_in.at[1, c, low], qa_recv.at[1, c])
        await_bytes(quart_in.at[0, c, low], qb_recv.at[0, c])
        await_bytes(quart_in.at[1, c, high], qb_recv.at[1, c])
        part[x, c] = (
            part[x, c].astype(F32) + quart_in[0, c].astype(F32) + quart_in[1, c].astype(F32)
        ).astype(BF16)

        @pl.when(c < nz)
        def _():
            home_z = (z + nz - dz_of(c)) % nz

            @pl.loop(jnp.where(c == 0, 1, 0), nk)
            def _(k):
                k_home = (k_own + k) % nk
                pltpu.make_async_remote_copy(
                    part.at[x, c, slot_rows(k_home)],
                    ret.at[slot_rows(e)],
                    ret_send.at[c],
                    ret_recv,
                    device_id=(home_z * nk + k_home, x),
                    device_id_type=MESH,
                ).start()

    def multiply(c):
        gate = jnp.zeros((chunk_rows, wg.shape[1]), F32)
        up = jnp.zeros((chunk_rows, wg.shape[1]), F32)
        for q in range(nx):
            rows_q = arr[q, c]
            gate = gate + dot(rows_q, wg[q * quarter : (q + 1) * quarter, :])
            up = up + dot(rows_q, wu[q * quarter : (q + 1) * quarter, :])
        hidden = (gate * jax.nn.sigmoid(gate) * up).astype(BF16)
        for q in range(nx):
            part[q, c] = dot(hidden, wd[:, q * quarter : (q + 1) * quarter]).astype(BF16)
        half_sends(c)
        quarter_sends(c)

    near_step = nz // 2 + 1
    each = max(1, 2 * nx // nz)

    def planes(turn):
        first = jnp.where(turn <= nz // 2, turn - 1, 2 * turn - nz // 2 - 2)
        return first, jnp.minimum(jnp.where(turn <= nz // 2, turn, first + 2), z + 1)

    last_turn = nz // 2 + nz // 4

    @pl.loop(0, nz + 1)
    def _(step):
        @pl.when(step >= 3)
        def _():
            pass_sums(step - 2)


        @pl.when(step >= 4)
        def _():
            finish(step - 3)


        @pl.when(step >= 2)
        def _():
            c = step - 1

            @pl.when(c == 1)
            def _():
                for load in loads[:3]:
                    load.wait()

            await_bytes(arr.at[far, c, low], fw_recv.at[0, c])
            await_bytes(arr.at[far, c, high], fw_recv.at[1, c])
            multiply(c)

        @pl.when((step >= 1) & (step < nz))
        def _():
            c = step
            await_bytes(arr.at[left, c], ag_recv.at[0, c])
            send(arr.at[left, c, low], arr.at[left, c, low], fw_send.at[0, c], fw_recv.at[0, c], right)
            await_bytes(arr.at[right, c], ag_recv.at[1, c])
            send(arr.at[right, c, high], arr.at[right, c, high], fw_send.at[1, c], fw_recv.at[1, c], left)

        @pl.when(step < nz - 1)
        def _():
            c = step + 1
            await_bytes(arr.at[x, c], a2a_recv.at[c])
            send(arr.at[x, c], arr.at[x, c], ag_send.at[0, c], ag_recv.at[0, c], right)
            send(arr.at[x, c], arr.at[x, c], ag_send.at[1, c], ag_recv.at[1, c], left)

        @pl.when(step == near_step)
        def _():
            await_bytes(arr.at[:, 0, first_rows], a2a_recv.at[0])
            multiply(0)

        @pl.when((step >= 2) & (step <= last_turn + 1))
        def _():
            @pl.loop(*planes(step - 1))
            def _(d):
                zs = z - d
                opposite = y_far * 2 + core
                await_bytes(kv.at[zs, opposite, b_low], kf_recv.at[0, d])
                await_bytes(kv.at[zs, opposite, b_high], kf_recv.at[1, d])
                send_block(kv.at[zs, opposite], ks_send.at[3, d], ks_recv.at[3, d], sibling)

        @pl.when((step >= 1) & (step <= last_turn))
        def _():
            @pl.loop(step, jnp.minimum(jnp.where(step == last_turn, nz, step + 1), z + 1))
            def _(d):
                await_bytes(kv.at[z - d, k_own], kz_recv.at[d])
                spread_column(d)

        @pl.when((step >= 1) & (step <= last_turn))
        def _():
            @pl.loop(*planes(step))
            def _(d):
                zs = z - d
                below = kv.at[zs, y_down * 2 + core]
                await_bytes(below, ky_recv.at[0, d])
                part_low = kv.at[zs, y_down * 2 + core, b_low]
                send_block(part_low, kf_send.at[0, d], kf_recv.at[0, d], up_dev)
                send_block(below, ks_send.at[1, d], ks_recv.at[1, d], sibling)
                above = kv.at[zs, y_up * 2 + core]
                await_bytes(above, ky_recv.at[1, d])
                part_high = kv.at[zs, y_up * 2 + core, b_high]
                send_block(part_high, kf_send.at[1, d], kf_recv.at[1, d], down_dev)
                send_block(above, ks_send.at[2, d], ks_recv.at[2, d], sibling)

        @pl.when(step + AHEAD + 1 < nz)
        def _():
            prepare(step + AHEAD + 1)
            dispatch(step + AHEAD + 1)

        @pl.when((step >= 1) & (step <= nx // each))
        def _():
            @pl.loop((step - 1) * each, step * each)
            def _(q):
                dispatch_near(q)

        @pl.when(step == near_step + 1)
        def _():
            pass_sums(0)

        @pl.when(step == near_step + 2)
        def _():
            finish(0)

        @pl.when((step >= 2) & (step <= last_turn + 1))
        def _():
            @pl.loop(*planes(step - 1))
            def _(d):
                zs = z - d
                for i, line_y in enumerate((y, y_down, y_up, y_far)):
                    await_bytes(kv.at[zs, line_y * 2 + 1 - core], ks_recv.at[i, d])

                @pl.loop(0, jnp.where(d == 0, k_own // 2, nk // 2))
                def _(p):
                    visit(zs, p, False)

                @pl.when(d == 0)
                def _():
                    visit(zs, k_own // 2, True)

    loads[3].wait()
    for h in range(heads):
        heads_ref[:, h * HD : (h + 1) * HD] = (acc_ref[h] / l_ref[h]).astype(BF16)
    for n in range(nx):
        mixed = dot(heads_ref[...], wo[:, n * quarter : (n + 1) * quarter]).astype(BF16)
        for q in range(nx):
            part[q, nz + n // 2, n % 2 * half : n % 2 * half + half, :] = mixed[
                q * half : (q + 1) * half, :
            ]
    if near_step + 2 > nz:
        finish(0)
    finish(nz - 2)
    pass_sums(nz - 1)
    half_sends(nz)
    half_sends(nz + 1)
    quarter_sends(nz)
    quarter_sends(nz + 1)
    finish(nz - 1)

    @pl.loop(nz, nz + 2)
    def _(c):
        pass_sums(c)

    @pl.loop(nz, nz + 2)
    def _(c):
        finish(c)

    for n in range(nx):
        mixed_ref[:, n * quarter : (n + 1) * quarter] = part[
            x, nz + n // 2, n % 2 * half : n % 2 * half + half, :
        ]

    ret[slot_rows(e), :] = part[x, 0, slot_rows(k_own), :]
    await_bytes(ret.at[pl.ds(0, (n_ep - 1) * CAP)], ret_recv)
    o_ref[...] = (dot(c_hi[...], ret[...]) + dot(c_lo[...], ret[...])).astype(BF16)

    await_bytes(part.at[x, 0, first_rows], ret_send.at[0])
    await_bytes(arr.at[:, 0, first_rows], a2a_send.at[0])

    @pl.loop(1, nz)
    def _(c):
        await_bytes(part.at[x, c], ret_send.at[c])
        await_bytes(arr.at[0, c], a2a_send.at[c])

    @pl.loop(0, nz)
    def _(c):
        @pl.when(c > 0)
        def _():
            for side in (0, 1):
                await_bytes(arr.at[0, c], ag_send.at[side, c])
                await_bytes(half_in.at[side, c], fw_send.at[side, c])

        @pl.when(c <= z)
        def _():
            block = kv.at[0, 0]

            @pl.when(z + 1 < nz)
            def _():
                await_bytes(block, kz_send.at[c])

            for side in (0, 1):
                await_bytes(block, ky_send.at[side, c])
                await_bytes(kv.at[0, 0, b_low], kf_send.at[side, c])
            for i in range(4):
                await_bytes(block, ks_send.at[i, c])

    @pl.loop(0, nz + 2)
    def _(c):
        for side in (0, 1):
            for sem in (hs_send, qa_send, qb_send):
                await_bytes(half_in.at[side, c], sem.at[side, c])


def per_device(
    queries, keys, values, cum_gates, out_proj,
    tokens, norm_gain, routes, route_weights, w_gate, w_up, w_down,
):
    rows, width = tokens.shape
    q_rows = queries.shape[0]
    heads = cum_gates.shape[1]
    n_ep, nx = lax.axis_size("ep"), lax.axis_size("tp")
    nk = NYC
    nz = n_ep // nk
    quarter = width // nx
    hidden = w_gate.shape[2]
    chunk = nk * CAP
    slots = n_ep * CAP
    block_rows = 2 * q_rows + 4 * (heads * q_rows // 128)
    vmem = pl.BlockSpec(memory_space=pltpu.VMEM)
    anywhere = pl.BlockSpec(memory_space=pl.ANY)
    dma = pltpu.SemaphoreType.DMA
    pair = dma((2, nz))
    more = dma((2, nz + 2))
    line = dma((nz + 1,))
    return pl.pallas_call(
        functools.partial(step_kernel, nz, nk, nx),
        out_shape=(
            jax.ShapeDtypeStruct((q_rows // nx, width), BF16),
            jax.ShapeDtypeStruct((rows, quarter), BF16),
        ),
        in_specs=[vmem] * 6 + [anywhere] * 6,
        out_specs=(vmem, vmem),
        scratch_shapes=[
            pltpu.VMEM((width, hidden), BF16),
            pltpu.VMEM((width, hidden), BF16),
            pltpu.VMEM((hidden, width), BF16),
            pltpu.VMEM(out_proj.shape, BF16),
            pltpu.VMEM((slots, quarter), BF16),
            pltpu.VMEM((nx, nz, chunk, quarter), BF16),
            pltpu.VMEM((nx, nz + 2, chunk, quarter), BF16),
            pltpu.VMEM((2, nz + 2, chunk // 2, quarter), BF16),
            pltpu.VMEM((2, nz + 2, chunk, quarter), BF16),
            pltpu.VMEM((slots, quarter), BF16),
            pltpu.VMEM((rows, slots), BF16),
            pltpu.VMEM((rows, slots), BF16),
            pltpu.VMEM((nz, nk, block_rows, HD), BF16),
            pltpu.VMEM((heads, q_rows, 1), F32),
            pltpu.VMEM((heads, q_rows, 1), F32),
            pltpu.VMEM((heads, q_rows, HD), F32),
            pltpu.VMEM((q_rows, heads * HD), BF16),
            pltpu.VMEM((rows, width), BF16),
            pltpu.VMEM((nx, chunk, quarter), BF16),
            dma((6,)),
            dma((nz,)), dma((nz,)),
            pair, pair, pair, pair,
            more, more, more, more, more, more,
            dma((nz,)),
            dma,
            line, line, pair, pair, pair, pair, dma((4, nz)), dma((4, nz)),
        ],
        compiler_params=pltpu.CompilerParams(
            collective_id=0, has_side_effects=True, vmem_limit_bytes=67043328
        ),
        cost_estimate=pl.CostEstimate(
            flops=100 * 10**9, bytes_accessed=10 * 2**20, transcendentals=0
        ),
    )(
        tokens, norm_gain[None], routes.T, route_weights.T, queries, cum_gates.T,
        w_gate[0], w_up[0], w_down[0], out_proj, keys, values,
    )


def solution(mesh):
    placed = (
        P("ep", "tp"), P("ep", "tp"), P("ep", "tp"), P("ep", "tp"), P("tp", None),
        P("ep", None), P(), P("ep", None), P("ep", None),
        P("ep", None, "tp"), P("ep", None, "tp"), P("ep", "tp", None),
    )
    return jax.shard_map(
        per_device,
        mesh=mesh,
        in_specs=placed,
        out_specs=(P(("ep", "tp"), None), P("ep", "tp")),
        check_vma=False,
    )
```

time: 199 us -> 193 us (0.970)
  the two profiles are of different devices: /device:TPU:224 before, /device:TPU:89 now
where the time goes in v4:
time: 193 us
  Pallas kernels  189 us (98%)
  local copies, waits for them, and re-layouts  3.54 us (2%)
    pallas_call x1, Pallas kernels, per_device(): pl.pallas_call(functools.partial(step_kernel, nz, nk, nx), out_shape=(jax...  189 us

profile of v4, /device:TPU:89, one launch (start us, length us, event | category | flops | bytes accessed | tf_op | source)
XLA Modules:
  0.0 193.1 jit_solution(17011064694095594337)
XLA Ops:
  0.6 188.9 %shard_map.131 = (bf16[64,4096]{1,0:T(8,128)(2,1)}, bf16[128,1024]{1,0:T(8,128)(2,1)}) custom-call(bf16[128,4096]{1,0:T(8,128)(2,1)} %tok_ref.1, f32[1,4096]{1,0:T(1,128)} %bitcast.10, s32[4,128]{1,0:T(4,128)} %bitcast.12, f32[4,128]{1,0:T(4,128)} %bitcast.13, bf16[256,512]{1,0:T(8,128)(2,1)} %q_ref.1, f32[4,256]{1,0:T(4,128)} %bitcast.11, ...), custom_call_target="tpu_custom_call" | custom-call | flops 99999997952 | bytes 10485760 | tf_op jit(solution)/shard_map/pallas_call | solution.py:543
  189.5 1.9 copy.16
  191.4 1.7 copy.17

commit v5 on v4

--- a/solution.py
+++ b/solution.py
@@ -16,7 +16,7 @@
 F32 = jnp.float32
 BF16 = jnp.bfloat16
 FLOOR = -1e30
-AHEAD = 2
+AHEAD = 3
 
 
 def iota(shape, dim):
@@ -115,11 +115,10 @@
         )
         return hit.astype(BF16)
 
-    order = [0, nz // 2]
-    for near in range(1, (nz + 1) // 2):
-        order[-1:-1] = [near, nz - near]
-    if nz > 4:
-        order[4], order[-1] = order[-1], order[4]
+    middle = [nz // 2]
+    for near in range(2, (nz + 1) // 2):
+        middle += [nz - near, near]
+    order = [0, 1] + middle[1:3] + middle[:1] + middle[3:] + [nz - 1]
 
     def dz_of(c):
         return sum(jnp.where(c == i, dz, 0) for i, dz in enumerate(order))
@@ -186,29 +185,31 @@
     dispatch(1)
     spread_column(0)
 
-    @pl.loop(2, min(AHEAD, nz - 1) + 1)
+    @pl.loop(2, min(AHEAD, nz - 2) + 1)
     def _(c):
         prepare(c)
         dispatch(c)
 
-    near = picks(z * chunk_rows)
-    for q in range(nx):
-        wide[q] = dot(near, norm_ref[:, q * quarter : (q + 1) * quarter]).astype(BF16)
-
-    def dispatch_near(q):
-        @pl.loop(1, nk)
+    below_z = (z + nz - 1) % nz
+    for i, to_z in enumerate((z, below_z)):
+        near = picks(to_z * chunk_rows)
+        for q in range(nx):
+            wide[i, q] = dot(near, norm_ref[:, q * quarter : (q + 1) * quarter]).astype(BF16)
+
+    def dispatch_wide(i, q, c, to_z):
+        @pl.loop(1 - i, nk)
         def _(k):
             k_dest = (k_own + k) % nk
             pltpu.make_async_remote_copy(
-                wide.at[q, slot_rows(k_dest)],
-                arr.at[q, 0, slot_rows(k_own)],
-                a2a_send.at[0],
-                a2a_recv.at[0],
-                device_id=(plane + k_dest, x),
+                wide.at[i, q, slot_rows(k_dest)],
+                arr.at[q, c, slot_rows(k_own)],
+                a2a_send.at[c],
+                a2a_recv.at[c],
+                device_id=(to_z * nk + k_dest, x),
                 device_id_type=MESH,
             ).start()
 
-    arr[:, 0, slot_rows(k_own), :] = wide[:, slot_rows(k_own), :]
+    arr[:, 0, slot_rows(k_own), :] = wide[0, :, slot_rows(k_own), :]
 
     same = (iota((rows, rows), 0) == iota((rows, rows), 1)).astype(BF16)
 
@@ -333,7 +334,7 @@
 
     last_turn = nz // 2 + nz // 4
 
-    @pl.loop(0, nz + 1)
+    @pl.loop(0, nz)
     def _(step):
         @pl.when(step >= 3)
         def _():
@@ -358,7 +359,7 @@
             await_bytes(arr.at[far, c, high], fw_recv.at[1, c])
             multiply(c)
 
-        @pl.when((step >= 1) & (step < nz))
+        @pl.when((step >= 1) & (step < nz - 1))
         def _():
             c = step
             await_bytes(arr.at[left, c], ag_recv.at[0, c])
@@ -366,12 +367,13 @@
             await_bytes(arr.at[right, c], ag_recv.at[1, c])
             send(arr.at[right, c, high], arr.at[right, c, high], fw_send.at[1, c], fw_recv.at[1, c], left)
 
-        @pl.when(step < nz - 1)
-        def _():
-            c = step + 1
-            await_bytes(arr.at[x, c], a2a_recv.at[c])
-            send(arr.at[x, c], arr.at[x, c], ag_send.at[0, c], ag_recv.at[0, c], right)
-            send(arr.at[x, c], arr.at[x, c], ag_send.at[1, c], ag_recv.at[1, c], left)
+        @pl.when(step < nz - 3)
+        def _():
+            @pl.loop(jnp.where(step == 0, 1, step + 2), step + 3)
+            def _(c):
+                await_bytes(arr.at[x, c], a2a_recv.at[c])
+                send(arr.at[x, c], arr.at[x, c], ag_send.at[0, c], ag_recv.at[0, c], right)
+                send(arr.at[x, c], arr.at[x, c], ag_send.at[1, c], ag_recv.at[1, c], left)
 
         @pl.when(step == near_step)
         def _():
@@ -411,7 +413,7 @@
                 send_block(part_high, kf_send.at[1, d], kf_recv.at[1, d], down_dev)
                 send_block(above, ks_send.at[2, d], ks_recv.at[2, d], sibling)
 
-        @pl.when(step + AHEAD + 1 < nz)
+        @pl.when(step + AHEAD + 1 < nz - 1)
         def _():
             prepare(step + AHEAD + 1)
             dispatch(step + AHEAD + 1)
@@ -420,7 +422,13 @@
         def _():
             @pl.loop((step - 1) * each, step * each)
             def _(q):
-                dispatch_near(q)
+                dispatch_wide(0, q, 0, z)
+
+        @pl.when((step >= 2) & (step <= nx // each + 1))
+        def _():
+            @pl.loop((step - 2) * each, (step - 1) * each)
+            def _(q):
+                dispatch_wide(1, q, nz - 1, below_z)
 
         @pl.when(step == near_step + 1)
         def _():
@@ -429,6 +437,11 @@
         @pl.when(step == near_step + 2)
         def _():
             finish(0)
+
+        @pl.when(step == nz - 1)
+        def _():
+            await_bytes(arr.at[:, nz - 1], a2a_recv.at[nz - 1])
+            multiply(nz - 1)
 
         @pl.when((step >= 2) & (step <= last_turn + 1))
         def _():
@@ -455,14 +468,14 @@
             part[q, nz + n // 2, n % 2 * half : n % 2 * half + half, :] = mixed[
                 q * half : (q + 1) * half, :
             ]
-    if near_step + 2 > nz:
-        finish(0)
-    finish(nz - 2)
+    pass_sums(nz - 2)
+    finish(nz - 3)
     pass_sums(nz - 1)
     half_sends(nz)
     half_sends(nz + 1)
     quarter_sends(nz)
     quarter_sends(nz + 1)
+    finish(nz - 2)
     finish(nz - 1)
 
     @pl.loop(nz, nz + 2)
@@ -483,16 +496,18 @@
     o_ref[...] = (dot(c_hi[...], ret[...]) + dot(c_lo[...], ret[...])).astype(BF16)
 
     await_bytes(part.at[x, 0, first_rows], ret_send.at[0])
+    await_bytes(part.at[x, nz - 1], ret_send.at[nz - 1])
+    await_bytes(arr.at[:, nz - 1], a2a_send.at[nz - 1])
     await_bytes(arr.at[:, 0, first_rows], a2a_send.at[0])
 
-    @pl.loop(1, nz)
+    @pl.loop(1, nz - 1)
     def _(c):
         await_bytes(part.at[x, c], ret_send.at[c])
         await_bytes(arr.at[0, c], a2a_send.at[c])
 
     @pl.loop(0, nz)
     def _(c):
-        @pl.when(c > 0)
+        @pl.when((c > 0) & (c < nz - 1))
         def _():
             for side in (0, 1):
                 await_bytes(arr.at[0, c], ag_send.at[side, c])
@@ -567,7 +582,7 @@
             pltpu.VMEM((heads, q_rows, HD), F32),
             pltpu.VMEM((q_rows, heads * HD), BF16),
             pltpu.VMEM((rows, width), BF16),
-            pltpu.VMEM((nx, chunk, quarter), BF16),
+            pltpu.VMEM((2, nx, chunk, quarter), BF16),
             dma((6,)),
             dma((nz,)), dma((nz,)),
             pair, pair, pair, pair,

time: 193 us -> 184 us (0.953)
  the two profiles are of different devices: /device:TPU:89 before, /device:TPU:224 now
where the time goes in v5:
time: 184 us
  Pallas kernels  179 us (97%)
  local copies, waits for them, and re-layouts  3.54 us (2%)
    pallas_call x1, Pallas kernels, per_device(): pl.pallas_call(functools.partial(step_kernel, nz, nk, nx), out_shape=(jax...  179 us

profile of v5, /device:TPU:224, one launch (start us, length us, event | category | flops | bytes accessed | tf_op | source)
XLA Modules:
  0.0 183.6 jit_solution(7626393243215978548)
XLA Ops:
  0.6 179.4 %shard_map.131 = (bf16[64,4096]{1,0:T(8,128)(2,1)}, bf16[128,1024]{1,0:T(8,128)(2,1)}) custom-call(bf16[128,4096]{1,0:T(8,128)(2,1)} %tok_ref.1, f32[1,4096]{1,0:T(1,128)} %bitcast.10, s32[4,128]{1,0:T(4,128)} %bitcast.12, f32[4,128]{1,0:T(4,128)} %bitcast.13, bf16[256,512]{1,0:T(8,128)(2,1)} %q_ref.1, f32[4,256]{1,0:T(4,128)} %bitcast.11, ...), custom_call_target="tpu_custom_call" | custom-call | flops 99999997952 | bytes 10485760 | tf_op jit(solution)/shard_map/pallas_call | solution.py:558
  180.1 1.9 %copy.16 = bf16[64,4096]{1,0:T(8,128)(2,1)} copy(bf16[64,4096]{1,0:T(8,128)(2,1)} %get-tuple-element.4) | data formatting | bytes 1048576
  181.9 1.7 copy.17

commit v6 on v5

--- a/solution.py
+++ b/solution.py
@@ -118,7 +118,7 @@
     middle = [nz // 2]
     for near in range(2, (nz + 1) // 2):
         middle += [nz - near, near]
-    order = [0, 1] + middle[1:3] + middle[:1] + middle[3:] + [nz - 1]
+    order = [0, 1] + middle[1:] + middle[:1] + [nz - 1]
 
     def dz_of(c):
         return sum(jnp.where(c == i, dz, 0) for i, dz in enumerate(order))
@@ -325,12 +325,29 @@
         half_sends(c)
         quarter_sends(c)
 
+    def flash_planes(first, end):
+        @pl.loop(first, end)
+        def _(d):
+            zs = z - d
+            for i, line_y in enumerate((y, y_down, y_up, y_far)):
+                await_bytes(kv.at[zs, line_y * 2 + 1 - core], ks_recv.at[i, d])
+
+            @pl.loop(0, jnp.where(d == 0, k_own // 2, nk // 2))
+            def _(p):
+                visit(zs, p, False)
+
+            @pl.when(d == 0)
+            def _():
+                visit(zs, k_own // 2, True)
+
     near_step = nz // 2 + 1
     each = max(1, 2 * nx // nz)
 
     def planes(turn):
-        first = jnp.where(turn <= nz // 2, turn - 1, 2 * turn - nz // 2 - 2)
-        return first, jnp.minimum(jnp.where(turn <= nz // 2, turn, first + 2), z + 1)
+        mid = nz // 2
+        first = turn - 1 + jnp.where(turn > mid, 1, 0)
+        end = turn + jnp.where(turn >= mid, 1, 0) + jnp.where(turn > mid + 1, 1, 0)
+        return first, jnp.minimum(end, z + 1)
 
     last_turn = nz // 2 + nz // 4
 
@@ -366,14 +383,6 @@
             send(arr.at[left, c, low], arr.at[left, c, low], fw_send.at[0, c], fw_recv.at[0, c], right)
             await_bytes(arr.at[right, c], ag_recv.at[1, c])
             send(arr.at[right, c, high], arr.at[right, c, high], fw_send.at[1, c], fw_recv.at[1, c], left)
-
-        @pl.when(step < nz - 3)
-        def _():
-            @pl.loop(jnp.where(step == 0, 1, step + 2), step + 3)
-            def _(c):
-                await_bytes(arr.at[x, c], a2a_recv.at[c])
-                send(arr.at[x, c], arr.at[x, c], ag_send.at[0, c], ag_recv.at[0, c], right)
-                send(arr.at[x, c], arr.at[x, c], ag_send.at[1, c], ag_recv.at[1, c], left)
 
         @pl.when(step == near_step)
         def _():
@@ -445,19 +454,22 @@
 
         @pl.when((step >= 2) & (step <= last_turn + 1))
         def _():
-            @pl.loop(*planes(step - 1))
-            def _(d):
-                zs = z - d
-                for i, line_y in enumerate((y, y_down, y_up, y_far)):
-                    await_bytes(kv.at[zs, line_y * 2 + 1 - core], ks_recv.at[i, d])
-
-                @pl.loop(0, jnp.where(d == 0, k_own // 2, nk // 2))
-                def _(p):
-                    visit(zs, p, False)
-
-                @pl.when(d == 0)
-                def _():
-                    visit(zs, k_own // 2, True)
+            first, end = planes(step - 1)
+            flash_planes(first, jnp.where(step == nz - 1, jnp.minimum(first + 1, end), end))
+
+        @pl.when(step == nz - 1)
+        def _():
+            pass_sums(nz - 2)
+            finish(nz - 3)
+            flash_planes(nz - 1, z + 1)
+
+        @pl.when(step < nz - 3)
+        def _():
+            @pl.loop(jnp.where(step == 0, 1, step + 2), step + 3)
+            def _(c):
+                await_bytes(arr.at[x, c], a2a_recv.at[c])
+                send(arr.at[x, c], arr.at[x, c], ag_send.at[0, c], ag_recv.at[0, c], right)
+                send(arr.at[x, c], arr.at[x, c], ag_send.at[1, c], ag_recv.at[1, c], left)
 
     loads[3].wait()
     for h in range(heads):
@@ -468,8 +480,6 @@
             part[q, nz + n // 2, n % 2 * half : n % 2 * half + half, :] = mixed[
                 q * half : (q + 1) * half, :
             ]
-    pass_sums(nz - 2)
-    finish(nz - 3)
     pass_sums(nz - 1)
     half_sends(nz)
     half_sends(nz + 1)

time: 184 us -> 177 us (0.962)
  Pallas kernels: 179 us -> 173 us
    pallas_call x1, Pallas kernels: 179 us -> 173 us  [per_device(): pl.pallas_call(functools.partial(step_kernel, nz, nk, nx), out_shape=(jax...]
where the time goes in v6:
time: 177 us
  Pallas kernels  173 us (98%)
  local copies, waits for them, and re-layouts  3.54 us (2%)
    pallas_call x1, Pallas kernels, per_device(): pl.pallas_call(functools.partial(step_kernel, nz, nk, nx), out_shape=(jax...  173 us

profile of v6, /device:TPU:224, one launch (start us, length us, event | category | flops | bytes accessed | tf_op | source)
XLA Modules:
  0.0 177.1 jit_solution(6492751815073311217)
XLA Ops:
  0.6 172.9 %shard_map.131 = (bf16[64,4096]{1,0:T(8,128)(2,1)}, bf16[128,1024]{1,0:T(8,128)(2,1)}) custom-call(bf16[128,4096]{1,0:T(8,128)(2,1)} %tok_ref.1, f32[1,4096]{1,0:T(1,128)} %bitcast.10, s32[4,128]{1,0:T(4,128)} %bitcast.12, f32[4,128]{1,0:T(4,128)} %bitcast.13, bf16[256,512]{1,0:T(8,128)(2,1)} %q_ref.1, f32[4,256]{1,0:T(4,128)} %bitcast.11, ...), custom_call_target="tpu_custom_call" | custom-call | flops 99999997952 | bytes 10485760 | tf_op jit(solution)/shard_map/pallas_call | solution.py:568
  173.5 1.9 %copy.16 = bf16[64,4096]{1,0:T(8,128)(2,1)} copy(bf16[64,4096]{1,0:T(8,128)(2,1)} %get-tuple-element.4) | data formatting | bytes 1048576
  175.4 1.7 copy.17

commit v7 on v6

--- a/solution.py
+++ b/solution.py
@@ -544,6 +544,11 @@
                 await_bytes(half_in.at[side, c], sem.at[side, c])
 
 
+def put_out(a_ref, b_ref, a_out, b_out):
+    a_out[...] = a_ref[...]
+    b_out[...] = b_ref[...]
+
+
 def per_device(
     queries, keys, values, cum_gates, out_proj,
     tokens, norm_gain, routes, route_weights, w_gate, w_up, w_down,
@@ -565,7 +570,7 @@
     pair = dma((2, nz))
     more = dma((2, nz + 2))
     line = dma((nz + 1,))
-    return pl.pallas_call(
+    results = pl.pallas_call(
         functools.partial(step_kernel, nz, nk, nx),
         out_shape=(
             jax.ShapeDtypeStruct((q_rows // nx, width), BF16),
@@ -611,6 +616,12 @@
         tokens, norm_gain[None], routes.T, route_weights.T, queries, cum_gates.T,
         w_gate[0], w_up[0], w_down[0], out_proj, keys, values,
     )
+    return pl.pallas_call(
+        put_out,
+        out_shape=tuple(jax.ShapeDtypeStruct(r.shape, r.dtype) for r in results),
+        in_specs=[vmem] * 2,
+        out_specs=(vmem, vmem),
+    )(*results)
 
 
 def solution(mesh):

time: 177 us -> 176 us (level)
  local copies, waits for them, and re-layouts: 3.54 us -> 0 us
  Pallas kernels: 173 us -> 175 us
    unnamed x2 -> x0, local copies, waits for them, and re-layouts: 3.54 us -> none
    pallas_call x0 -> x1, Pallas kernels: none -> 2.02 us  [per_device(): pl.pallas_call(put_out, out_shape=tuple((jax.ShapeDtypeStruct(r.shape, r....]
where the time goes in v7:
time: 176 us
  Pallas kernels  175 us (99%)
    pallas_call x1, Pallas kernels, per_device(): pl.pallas_call(functools.partial(step_kernel, nz, nk, nx), out_shape=(jax...  173 us

profile of v7, /device:TPU:224, one launch (start us, length us, event | category | flops | bytes accessed | tf_op | source)
XLA Modules:
  0.0 175.6 jit_solution(1517965671440762502)
XLA Ops:
  0.6 172.9 %shard_map.131 = (bf16[64,4096]{1,0:T(8,128)(2,1)}, bf16[128,1024]{1,0:T(8,128)(2,1)}) custom-call(bf16[128,4096]{1,0:T(8,128)(2,1)} %tok_ref.1, f32[1,4096]{1,0:T(1,128)} %bitcast.10, s32[4,128]{1,0:T(4,128)} %bitcast.12, f32[4,128]{1,0:T(4,128)} %bitcast.13, bf16[256,512]{1,0:T(8,128)(2,1)} %q_ref.1, f32[4,256]{1,0:T(4,128)} %bitcast.11, ...), custom_call_target="tpu_custom_call" | custom-call | flops 99999997952 | bytes 10485760 | tf_op jit(solution)/shard_map/pallas_call | solution.py:573
  173.5 2.0 %shard_map.132 = (bf16[64,4096]{1,0:T(8,128)(2,1)}, bf16[128,1024]{1,0:T(8,128)(2,1)}) custom-call(bf16[64,4096]{1,0:T(8,128)(2,1)} %get-tuple-element.4.a_ref, bf16[128,1024]{1,0:T(8,128)(2,1)} %get-tuple-element.5.b_ref), custom_call_target="tpu_custom_call" | custom-call | tf_op jit(solution)/shard_map/pallas_call | solution.py:619
